TPU v7x, 256 devices: a whole 4x4x8 slice. The times are simulated.
256 devices in a mesh: ep: 64 (over z, x, core), tp: 4 (over y).
Axes of the slice: x: 4, y: 4, z: 8, core: 2. Of those that a mesh axis runs over, the one named last changes fastest.
Arguments:
- tokens: bfloat16 [2048, 2048], P('ep'), may hold values from -6 to 6
- norm_gain_attn: float32 [2048], replicated, may hold values from 0.1 to 1.9
- w_query: bfloat16 [2048, 2048], P('ep', 'tp'), may hold values from -0.125 to 0.125
- w_key: bfloat16 [2048, 256], P('ep', 'tp'), may hold values from -0.125 to 0.125
- w_value: bfloat16 [2048, 256], P('ep', 'tp'), may hold values from -0.125 to 0.125
- w_forget: bfloat16 [2048, 32], P(None, 'tp'), may hold values from -0.125 to 0.125
- forget_bias: float32 [32], P('tp'), may hold values from -1 to 3
- cache_keys: bfloat16 [2048, 256, 1024], P('ep', 'tp'), may hold values from -64 to 64
- cache_values: bfloat16 [2048, 256, 1024], P('ep', 'tp'), may hold values from -6 to 6
- cache_logcum: float32 [2048, 32, 1024], P('ep', 'tp'), may hold values from -2048 to 0, as said below
- lengths: int32 [2048], P('ep'), may hold values from 1 to 1023, as said below
- w_out: bfloat16 [2048, 2048], P('tp'), may hold values from -0.125 to 0.125
- norm_gain_mix: float32 [2048], replicated, may hold values from 0.1 to 1.9
- norm_gain_ffn: float32 [2048], replicated, may hold values from 0.1 to 1.9
- expert_gate: bfloat16 [2048, 65536], P(None, ('ep', 'tp')), may hold values from -0.125 to 0.125
- expert_up: bfloat16 [2048, 65536], P(None, ('ep', 'tp')), may hold values from -0.125 to 0.125
- expert_down: bfloat16 [65536, 2048], P(('ep', 'tp')), may hold values from -0.09375 to 0.09375
- routes: int32 [2048, 2], P('ep'), may hold values from 0 to 15, all different within a row; in each aligned block of 32 rows (0 to 31, 32 to 63, ...) at most 8 rows name the same one
- route_weights: float32 [2048, 2], P('ep'), may hold values from 0.2 to 1
Outputs:
- layer_out: bfloat16 [2048, 2048], P('ep', 'tp')
- new_keys: bfloat16 [2048, 256], P('ep', 'tp')
- new_values: bfloat16 [2048, 256], P('ep', 'tp')
- new_log_gate: float32 [2048, 32], P('ep', 'tp')
Inputs may be any that keep to these rules, and one draw needn't show every extreme that they name: `routes`: each row names 2 different experts. Within the rows of one index of ep no expert is named by more than 8 rows, and in every draw some expert is named by exactly 8 rows of some index. `lengths`: some sequence has 1023 cached positions in every draw. `cache_logcum`: never rising along positions (the last dimension).
All inputs are finite; a program needn't handle non-finite values.
Results may differ from a plain program's by a relative error of at most 0.013.
Values may be sent and summed in bfloat16 or wider, within the bound.
No kernel may reach another device: no remote copies, remote signals or barrier semaphores. Data moves between devices by JAX's collectives and lax.ppermute only.
A program may use at most 64 MiB of HBM per device.

v0:
```python
import functools

import jax
import jax.numpy as jnp
from jax import lax
from jax.experimental import pallas as pl
from jax.experimental.pallas import tpu as pltpu
from jax.sharding import Mesh, PartitionSpec as P


HEAD_DIM = 64
EXPERTS = 16
CAP = 8
EPSILON = 1e-06
MASKED = -1e30
EP = ("z", "x", "c")
F32 = jnp.float32
BF16 = jnp.bfloat16


def shifted(value, axis, step):
    n = lax.axis_size(axis)
    return lax.ppermute(value, axis, [(i, (i + step) % n) for i in range(n)])


def exchange(blocks, axis):
    return lax.all_to_all(blocks, axis, split_axis=0, concat_axis=0, tiled=True)


def inv_rms(field):
    return lax.rsqrt(jnp.mean(field * field, axis=-1, keepdims=True) + EPSILON)


def expert_kernel(nx, rows_ref, gate_ref, up_ref, down_ref, out_ref):
    blocks, part, width = rows_ref.shape
    ny = blocks // nx
    gate = up = None
    for y in range(ny):
        taken = jnp.concatenate([rows_ref[x * ny + y] for x in range(nx)], axis=0)
        deep = pl.ds(y * width, width)
        g = jnp.dot(taken, gate_ref[deep, :], preferred_element_type=F32)
        u = jnp.dot(taken, up_ref[deep, :], preferred_element_type=F32)
        gate, up = (g, u) if gate is None else (gate + g, up + u)
    hidden = (gate / (1.0 + jnp.exp(-gate)) * up).astype(BF16)
    for y in range(ny):
        back = jnp.dot(hidden, down_ref[:, pl.ds(y * width, width)], preferred_element_type=F32)
        back = back.astype(BF16)
        for x in range(nx):
            out_ref[x * ny + y] = back[x * part : (x + 1) * part]


def expert_rows(blocks, gate, up, down, nx):
    return pl.pallas_call(
        functools.partial(expert_kernel, nx),
        out_shape=jax.ShapeDtypeStruct(blocks.shape, BF16),
        in_specs=[pl.BlockSpec(memory_space=pltpu.VMEM)] * 4,
        out_specs=pl.BlockSpec(memory_space=pltpu.VMEM),
        compiler_params=pltpu.CompilerParams(vmem_limit_bytes=16 * 2**20),
        cost_estimate=pl.CostEstimate(
            flops=2 * blocks.size * 3 * gate.shape[1],
            bytes_accessed=4 * blocks.size + 6 * gate.size,
            transcendentals=0,
        ),
    )(blocks, gate, up, down)


def attend_kernel(
    together,
    tokens_ref,
    gain_ref,
    forget_ref,
    bias_ref,
    own_ref,
    pieces_refs,
    cum_ref,
    length_ref,
    keys_ref,
    values_ref,
    out_w_ref,
    mix_ref,
    key_ref,
    value_ref,
    gate_ref,
    q_s,
    own_s,
    gate_s,
    weight_s,
    heads_s,
    keys_s,
    values_s,
    sems,
):
    rows = tokens_ref.shape[0]
    _, head_dim, span_len = keys_ref.shape
    _, group, _ = q_s.shape
    cols = group * head_dim
    scale = HEAD_DIM ** (-0.5)
    copies = []
    for step in range(rows // together):
        some = pl.ds(step * together, together)
        copies.append(
            (
                pltpu.make_async_copy(keys_ref.at[some], keys_s.at[some], sems.at[0, step]),
                pltpu.make_async_copy(values_ref.at[some], values_s.at[some], sems.at[1, step]),
            )
        )
        for copy in copies[step]:
            copy.start()

    tokens = tokens_ref[...].astype(F32)
    scale_attn = lax.rsqrt(jnp.mean(tokens * tokens, axis=1, keepdims=True) + EPSILON)
    normed = (tokens * scale_attn * gain_ref[...]).astype(BF16)
    logits = lax.dot_general(
        normed, forget_ref[...], (((1,), (1,)), ((), ())), preferred_element_type=F32
    )
    logits = logits + bias_ref[...]
    gate = jnp.minimum(logits, 0.0) - jnp.log1p(jnp.exp(-jnp.abs(logits)))
    gate_ref[...] = gate
    projected = own_ref[...]
    for ref in pieces_refs:
        projected = projected + ref[...].astype(F32)
    projected = projected * scale_attn
    new_key = projected[:, cols : cols + head_dim].astype(BF16)
    new_value = projected[:, cols + head_dim : cols + 2 * head_dim].astype(BF16)
    key_ref[...] = new_key
    value_ref[...] = new_value

    query = projected[:, :cols].astype(BF16).astype(F32)
    at_head = lax.broadcasted_iota(jnp.int32, (rows, group, cols), 1)
    of_head = lax.shift_right_logical(
        lax.broadcasted_iota(jnp.int32, (rows, group, cols), 2), head_dim.bit_length() - 1
    )
    on_head = at_head == of_head
    spread = jnp.where(on_head, jnp.broadcast_to(query[:, None, :], (rows, group, cols)), 0.0)
    spread = spread.reshape(rows * group, cols).astype(BF16)
    fold = (
        lax.bitwise_and(lax.broadcasted_iota(jnp.int32, (cols, head_dim), 0), head_dim - 1)
        == lax.broadcasted_iota(jnp.int32, (cols, head_dim), 1)
    )
    fold = jnp.where(fold, 1.0, 0.0).astype(BF16)
    by_head = jnp.dot(spread, fold, preferred_element_type=F32).reshape(rows, group, head_dim)
    q_s[...] = by_head
    own_s[...] = (
        jnp.sum(by_head * new_key.astype(F32)[:, None, :], axis=2, keepdims=True) * scale
    )
    same = lax.broadcasted_iota(jnp.int32, (rows, group, group), 1) == lax.broadcasted_iota(
        jnp.int32, (rows, group, group), 2
    )
    gate_s[...] = jnp.sum(jnp.where(same, gate[:, None, :], 0.0), axis=2, keepdims=True)
    places = lax.broadcasted_iota(jnp.int32, (group, span_len), 1)

    for step in range(rows // together):
        for copy in copies[step]:
            copy.wait()
        for k in range(together):
            b = step * together + k
            length = length_ref[b]
            scores = jnp.dot(q_s[b].astype(BF16), keys_s[b], preferred_element_type=F32) * scale
            cum = cum_ref[b]
            last = jnp.sum(jnp.where(places == length - 1, cum, 0.0), axis=1, keepdims=True)
            past = jnp.where(places < length, scores + ((last + gate_s[b]) - cum), MASKED)
            own = own_s[b]
            peak = jnp.maximum(jnp.max(past, axis=1, keepdims=True), own)
            past_exp = jnp.exp(past - peak)
            own_exp = jnp.exp(own - peak)
            total = jnp.sum(past_exp, axis=1, keepdims=True) + own_exp
            weight = (past_exp / total).astype(BF16)
            weight_s[b] = own_exp / total
            heads_s[b] = lax.dot_general(
                weight, values_s[b], (((1,), (1,)), ((), ())), preferred_element_type=F32
            )
    own_weight = weight_s[...].astype(BF16).astype(F32)
    heads = heads_s[...] + own_weight * new_value.astype(F32)[:, None, :]
    heads = heads.reshape(rows * group, head_dim).astype(BF16)
    wide = lax.dot_general(heads, fold, (((1,), (1,)), ((), ())), preferred_element_type=F32)
    wide = jnp.where(on_head, wide.reshape(rows, group, cols), 0.0)
    heads_out = jnp.sum(wide, axis=1).astype(BF16)
    mix_ref[...] = jnp.dot(heads_out, out_w_ref[...], preferred_element_type=F32).astype(BF16)


def attend(tokens, gain, forget, bias, own, pieces, cum, lengths, keys, values, out_w):
    rows, width = tokens.shape
    group, head_dim = cum.shape[1], keys.shape[1]
    in_vmem = pl.BlockSpec(memory_space=pltpu.VMEM)
    in_smem = pl.BlockSpec(memory_space=pltpu.SMEM)
    in_hbm = pl.BlockSpec(memory_space=pltpu.HBM)
    one = jax.ShapeDtypeStruct((rows, head_dim), BF16)
    together = 8
    return pl.pallas_call(
        functools.partial(attend_kernel, together),
        out_shape=(
            jax.ShapeDtypeStruct((rows, width), BF16),
            one,
            one,
            jax.ShapeDtypeStruct((rows, group), F32),
        ),
        in_specs=[in_vmem] * 5
        + [[in_vmem] * len(pieces), in_vmem, in_smem, in_hbm, in_hbm, in_vmem],
        out_specs=(in_vmem,) * 4,
        scratch_shapes=[
            pltpu.VMEM((rows, group, head_dim), F32),
            pltpu.VMEM((rows, group, 1), F32),
            pltpu.VMEM((rows, group, 1), F32),
            pltpu.VMEM((rows, group, 1), F32),
            pltpu.VMEM((rows, group, head_dim), F32),
            pltpu.VMEM(keys.shape, BF16),
            pltpu.VMEM(values.shape, BF16),
            pltpu.SemaphoreType.DMA((2, rows // together)),
        ],
        compiler_params=pltpu.CompilerParams(vmem_limit_bytes=24 * 2**20),
        cost_estimate=pl.CostEstimate(
            flops=4 * keys.size * group + 2 * rows * out_w.size,
            bytes_accessed=4 * keys.size + 4 * cum.size + 2 * out_w.size,
            transcendentals=cum.size,
        ),
    )(tokens, gain, forget, bias, own, pieces, cum, lengths, keys, values, out_w)


def slots_kernel(routes_ref, weights_ref, selector_ref, weighing_ref):
    top, rows = routes_ref.shape
    named = [routes_ref[pl.ds(k, 1), :] for k in range(top)]
    experts = lax.broadcasted_iota(jnp.int32, (EXPERTS, rows), 0)
    hits = [jnp.where(experts == one, 1.0, 0.0) for one in named]
    both = sum(hits[1:], hits[0])
    before = lax.broadcasted_iota(jnp.int32, (rows, rows), 0) < lax.broadcasted_iota(
        jnp.int32, (rows, rows), 1
    )
    earlier = jnp.dot(
        both.astype(BF16), jnp.where(before, 1.0, 0.0).astype(BF16), preferred_element_type=F32
    )
    places = lax.broadcasted_iota(jnp.int32, (EXPERTS * CAP, rows), 0)
    chosen = jnp.zeros((EXPERTS * CAP, rows), F32)
    weighed = jnp.zeros((EXPERTS * CAP, rows), F32)
    for k in range(top):
        slot = jnp.sum(earlier * hits[k], axis=0, keepdims=True).astype(jnp.int32)
        there = jnp.where(places == named[k] * CAP + slot, 1.0, 0.0)
        chosen = chosen + there
        weighed = weighed + there * weights_ref[pl.ds(k, 1), :]
    selector_ref[...] = chosen.astype(BF16)
    weighing_ref[...] = weighed


def slots(routes, weights):
    in_vmem = pl.BlockSpec(memory_space=pltpu.VMEM)
    shape = (EXPERTS * CAP, routes.shape[1])
    return pl.pallas_call(
        slots_kernel,
        out_shape=(jax.ShapeDtypeStruct(shape, BF16), jax.ShapeDtypeStruct(shape, F32)),
        in_specs=[in_vmem] * 2,
        out_specs=(in_vmem,) * 2,
        compiler_params=pltpu.CompilerParams(vmem_limit_bytes=4 * 2**20),
    )(routes, weights)


def layer(
    tokens,
    norm_gain_attn,
    w_query,
    w_key,
    w_value,
    w_forget,
    forget_bias,
    cache_keys,
    cache_values,
    cache_logcum,
    lengths,
    w_out,
    norm_gain_mix,
    norm_gain_ffn,
    expert_gate,
    expert_up,
    expert_down,
    routes,
    route_weights,
):
    rows, width = tokens.shape
    nz, nx, nc, ny = (lax.axis_size(a) for a in ("z", "x", "c", "y"))
    ix, ic, iy = lax.axis_index("x"), lax.axis_index("c"), lax.axis_index("y")

    selector, weighing = slots(routes.T, route_weights.T)

    weights = jnp.concatenate((w_query, w_key, w_value), axis=1)
    cols = weights.shape[1]
    same_core = exchange(jnp.broadcast_to(weights, (nz, *weights.shape)), "z")
    other_core = shifted(same_core, "c", 1)
    deep = width // (nx * nc)
    scaled = (tokens.astype(F32) * norm_gain_attn).astype(BF16)
    scaled = scaled.reshape(rows, nz, nx, nc, width // (nz * nx * nc)).transpose(2, 3, 0, 1, 4)
    scaled = scaled.reshape(nx, nc, rows, deep)
    mine = [
        jnp.concatenate(
            [
                lax.dynamic_slice(
                    scaled, ((ix + s) % nx, (ic + k) % nc, 0, 0), (1, 1, rows, deep)
                )[0, 0]
                for k in range(nc)
            ],
            axis=1,
        )
        for s in range(nx)
    ]
    moved = [shifted(mine[s], "x", s) for s in range(1, nx)]
    part_tokens = jnp.concatenate([mine[0]] + moved, axis=0)
    partial = jnp.dot(
        part_tokens[:, :deep], same_core.reshape(deep, cols), preferred_element_type=F32
    ) + jnp.dot(part_tokens[:, deep:], other_core.reshape(deep, cols), preferred_element_type=F32)
    pieces = [
        shifted(partial[s * rows : (s + 1) * rows].astype(BF16), "x", nx - s)
        for s in range(1, nx)
    ]

    partial_mix, new_keys, new_values, new_log_gate = attend(
        tokens,
        norm_gain_attn.reshape(1, width),
        w_forget.T,
        forget_bias.reshape(1, -1),
        partial[:rows],
        pieces,
        cache_logcum,
        lengths,
        pltpu.with_memory_space_constraint(cache_keys, pltpu.HBM),
        pltpu.with_memory_space_constraint(cache_values, pltpu.HBM),
        w_out,
    )

    residual = tokens.astype(F32)
    others = [shifted(partial_mix, "y", s) for s in range(1, ny)]
    mix = partial_mix.astype(F32)
    for other in others:
        mix = mix + other.astype(F32)
    mixed_res = residual + mix * inv_rms(mix) * norm_gain_mix
    col_width = width // ny
    scale_ffn = inv_rms(mixed_res)
    residual_cols = lax.dynamic_slice_in_dim(mixed_res, iy * col_width, col_width, 1)
    gain_ffn_cols = lax.dynamic_slice_in_dim(norm_gain_ffn, iy * col_width, col_width, 0)
    ffn_cols = (residual_cols * scale_ffn * gain_ffn_cols).astype(BF16)

    packed = jnp.dot(selector, ffn_cols, preferred_element_type=F32).astype(BF16)
    local_experts = EXPERTS // nz
    spread = nx // local_experts
    on_z = exchange(packed.reshape(nz, local_experts * CAP, col_width), "z")
    on_z = on_z.reshape(nz, local_experts, CAP, col_width).transpose(1, 0, 2, 3)
    on_z = on_z.reshape(local_experts, 1, 1, nz * CAP, col_width)
    outgoing = jnp.broadcast_to(on_z, (local_experts, spread, ny, nz * CAP, col_width))
    own = exchange(outgoing.reshape(nx * ny, nz * CAP, col_width), ("x", "y"))
    other = shifted(own, "c", 1)
    own_part = expert_rows(own, expert_gate, expert_up, expert_down, nx)
    other_part = expert_rows(other, expert_gate, expert_up, expert_down, nx)
    both = own_part.astype(F32) + shifted(other_part, "c", 1).astype(F32)
    summed = exchange(both.astype(BF16), ("x", "y"))
    summed = summed.reshape(local_experts, spread * ny, nz, CAP, col_width).astype(F32)
    summed = jnp.sum(summed, axis=1).astype(BF16).transpose(1, 0, 2, 3)
    returned = exchange(summed.reshape(nz, local_experts * CAP, col_width), "z")
    returned = returned.reshape(EXPERTS * CAP, col_width)
    routed = lax.dot_general(
        weighing, returned.astype(F32), (((0,), (0,)), ((), ())), preferred_element_type=F32
    )
    layer_out = (residual_cols + routed).astype(BF16)
    return (layer_out, new_keys, new_values, new_log_gate)


def solution(mesh):
    chips = Mesh(mesh.devices.reshape(8, 4, 2, 4), ("z", "x", "c", "y"))
    everyone = ("z", "x", "c", "y")
    placed = (
        P(EP, None),
        P(),
        P(EP, "y"),
        P(EP, "y"),
        P(EP, "y"),
        P(None, "y"),
        P("y"),
        P(EP, "y", None),
        P(EP, "y", None),
        P(EP, "y", None),
        P(EP),
        P("y", None),
        P(),
        P(),
        P(None, everyone),
        P(None, everyone),
        P(everyone, None),
        P(EP, None),
        P(EP, None),
    )
    return jax.shard_map(
        layer,
        mesh=chips,
        in_specs=placed,
        out_specs=(P(EP, "y"), P(EP, "y"), P(EP, "y"), P(EP, "y")),
        check_vma=False,
    )
```

profile of v0, /device:TPU:1, one launch (start us, length us, event | category | flops | bytes accessed | tf_op | source)
XLA Modules:
  0.0 131.4 jit_solution(18051517188389956050)
XLA Ops:
  0.6 0.9 pad_maximum_fusion.1
  2.3 9.0 %all-to-all-start = ((bf16[8,32,640]{2,1,0:T(8,128)(2,1)}), bf16[8,32,640]{2,1,0:T(8,128)(2,1)}, u32[]{:S(2)}, u32[]{:S(2)}) async-start(bf16[8,32,640]{2,1,0:T(8,128)(2,1)} %broadcast_in_dim.6), calls=%async_computation | async-start | bytes 655360 | tf_op jit(solution)/shard_map/all_to_all | solution.py:27
  11.3 0.9 fusion.1
  12.6 0.9 copy.35
  13.5 1.6 %reshape.68 = bf16[4,2,32,256]{3,2,1,0:T(8,128)(2,1)S(1)} reshape(bf16[4,2,32,8,32]{4,3,2,1,0:T(8,128)(2,1)} %bitcast.56) | data formatting | bytes 262144 | tf_op jit(solution)/shard_map/reshape | solution.py:289
  15.2 1.3 collective-permute-start
  16.5 7.0 %all-to-all-done = bf16[8,32,640]{2,1,0:T(8,128)(2,1)} async-done(((bf16[8,32,640]{2,1,0:T(8,128)(2,1)}), bf16[8,32,640]{2,1,0:T(8,128)(2,1)}, u32[]{:S(2)}, u32[]{:S(2)}) %all-to-all-start) | async-done | bytes 327712 | tf_op jit(solution)/shard_map/all_to_all | solution.py:27
  23.5 2.1 %collective-permute-start.3 = (bf16[8,32,640]{2,1,0:T(8,128)(2,1)}, bf16[8,32,640]{2,1,0:T(8,128)(2,1)S(1)}, u32[]{:S(2)}, u32[]{:S(2)}) collective-permute-start(bf16[8,32,640]{2,1,0:T(8,128)(2,1)} %all-to-all-done), channel_id=1, source_target_pairs={{0,4},{4,0},{1,5},{5,1},{2,6},{6,2},{3,7},{7,3},{8,12},{12,8},{9,1... | collective-permute-start | bytes 983048 | tf_op jit(solution)/shard_map/ppermute | solution.py:23
  25.6 2.7 %collective-permute-start.1 = (bf16[32,512]{1,0:T(8,128)(2,1)S(1)}, bf16[32,512]{1,0:T(8,128)(2,1)S(1)}, u32[]{:S(2)}, u32[]{:S(2)}) collective-permute-start(bf16[32,512]{1,0:T(8,128)(2,1)S(1)} %pad_maximum_fusion.3), channel_id=1, source_target_pairs={{0,16},{8,24},{16,0},{24,8},{1,17},{9,25},{17,1},{25,9},{2,18},{10... | collective-permute-start | bytes 98312 | tf_op jit(solution)/shard_map/ppermute | solution.py:23
  28.4 0.9 collective-permute-start.2
  29.9 1.2 collective-permute-done.2
  31.4 1.2 fusion.9
  32.6 0.9 collective-permute-start.6
  33.5 2.4 %collective-permute-start.5 = (bf16[32,640]{1,0:T(8,128)(2,1)S(1)}, bf16[32,640]{1,0:T(8,128)(2,1)S(1)}, u32[]{:S(2)}, u32[]{:S(2)}) collective-permute-start(bf16[32,640]{1,0:T(8,128)(2,1)S(1)} %get-tuple-element.31), channel_id=1, source_target_pairs={{0,16},{8,24},{16,0},{24,8},{1,17},{9,25},{17,1},{25,9},{2,18},{10... | collective-permute-start | bytes 122888 | tf_op jit(solution)/shard_map/ppermute | solution.py:23
  36.7 1.1 collective-permute-done.5.pieces_refs_1_
  37.9 1.2 collective-permute-done.4.pieces_refs_0_
  39.2 11.9 %shard_map.210 = (bf16[32,2048]{1,0:T(8,128)(2,1)S(1)}, bf16[32,64]{1,0:T(8,128)(2,1)}, bf16[32,64]{1,0:T(8,128)(2,1)}, f32[32,8]{1,0:T(8,128)S(1)}) custom-call(bf16[32,2048]{1,0:T(8,128)(2,1)S(1)} %copy-done.4, f32[1,2048]{1,0:T(1,128)S(1)} %bitcast.50, bf16[8,2048]{1,0:T(8,128)(2,1)S(1)} %bitcast.49, f32[1,8]{1,0:T(1,128)S(1)} %bitcast.53, ...), custom_call_target="tpu_custom_call" | custom-call | flops 134217728 | bytes 11534336 | tf_op jit(solution)/shard_map/pallas_call | solution.py:189
  51.1 2.8 %collective-permute-start.9 = (bf16[32,2048]{1,0:T(8,128)(2,1)S(1)}, bf16[32,2048]{1,0:T(8,128)(2,1)S(1)}, u32[]{:S(2)}, u32[]{:S(2)}) collective-permute-start(bf16[32,2048]{1,0:T(8,128)(2,1)S(1)} %get-tuple-element.10), channel_id=1, source_target_pairs={{0,3},{1,0},{2,1},{3,2},{4,7},{5,4},{6,5},{7,6},{8,11},{9,8},{10,9... | collective-permute-start | bytes 393224 | tf_op jit(solution)/shard_map/ppermute | solution.py:23
  55.8 1.4 %collective-permute-done.9 = bf16[32,2048]{1,0:T(8,128)(2,1)S(1)} collective-permute-done((bf16[32,2048]{1,0:T(8,128)(2,1)S(1)}, bf16[32,2048]{1,0:T(8,128)(2,1)S(1)}, u32[]{:S(2)}, u32[]{:S(2)}) %collective-permute-start.9) | collective-permute-done | bytes 131104 | tf_op jit(solution)/shard_map/ppermute | solution.py:23
  57.2 2.1 %collective-permute-done.8 = bf16[32,2048]{1,0:T(8,128)(2,1)S(1)} collective-permute-done((bf16[32,2048]{1,0:T(8,128)(2,1)S(1)}, bf16[32,2048]{1,0:T(8,128)(2,1)S(1)}, u32[]{:S(2)}, u32[]{:S(2)}) %collective-permute-start.8) | collective-permute-done | bytes 131104 | tf_op jit(solution)/shard_map/ppermute | solution.py:23
  59.3 1.3 collective-permute-done.7
  61.3 10.4 %all_to_all.25 = bf16[8,16,512]{2,1,0:T(8,128)(2,1)S(1)} all-to-all(bf16[8,16,512]{2,1,0:T(8,128)(2,1)S(1)} %bitcast.57), channel_id=1, replica_groups=mesh['z'=8,'x'=4,'c'=2,'y'=4] {'z'}, dimensions={0} | all-to-all | bytes 262144 | tf_op jit(solution)/shard_map/all_to_all | solution.py:27
  71.9 14.8 %all_to_all.26.rows_ref = bf16[16,64,512]{2,1,0:T(8,128)(2,1)S(1)} all-to-all(bf16[16,64,512]{2,1,0:T(8,128)(2,1)S(1)} %bitcast.55), channel_id=1, replica_groups=mesh['z'=8,'x'=4,'c'=2,'y'=4] {'x','y'}, dimensions={0} | all-to-all | bytes 2097152 | tf_op jit(solution)/shard_map/all_to_all | solution.py:27
  86.6 6.3 %collective-permute-start.10 = (bf16[16,64,512]{2,1,0:T(8,128)(2,1)S(1)}, bf16[16,64,512]{2,1,0:T(8,128)(2,1)S(1)}, u32[]{:S(2)}, u32[]{:S(2)}) collective-permute-start(bf16[16,64,512]{2,1,0:T(8,128)(2,1)S(1)} %all_to_all.26.rows_ref), channel_id=1, source_target_pairs={{0,4},{4,0},{1,5},{5,1},{2,6},{6,2},{3,7},{7,3},{8,12},{12,8},{9,1... | collective-permute-start | bytes 3145736 | tf_op jit(solution)/shard_map/ppermute | solution.py:23
  93.0 2.3 %collective-permute-done.10.rows_ref = bf16[16,64,512]{2,1,0:T(8,128)(2,1)S(1)} collective-permute-done((bf16[16,64,512]{2,1,0:T(8,128)(2,1)S(1)}, bf16[16,64,512]{2,1,0:T(8,128)(2,1)S(1)}, u32[]{:S(2)}, u32[]{:S(2)}) %collective-permute-start.10) | collective-permute-done | bytes 1048608 | tf_op jit(solution)/shard_map/ppermute | solution.py:23
  95.3 1.1 shard_map.213
  96.8 1.1 shard_map.212
  97.9 1.2 collective-permute-done.11
  99.5 19.0 %all_to_all.27 = bf16[16,64,512]{2,1,0:T(8,128)(2,1)S(1)} all-to-all(bf16[16,64,512]{2,1,0:T(8,128)(2,1)S(1)} %add_convert_fusion), channel_id=1, replica_groups=mesh['z'=8,'x'=4,'c'=2,'y'=4] {'x','y'}, dimensions={0} | all-to-all | bytes 2097152 | tf_op jit(solution)/shard_map/all_to_all | solution.py:27
  119.3 3.4 %all-to-all-start.4 = ((bf16[8,16,512]{2,1,0:T(8,128)(2,1)}), bf16[8,16,512]{2,1,0:T(8,128)(2,1)S(1)}, u32[]{:S(2)}, u32[]{:S(2)}) async-start(bf16[8,16,512]{2,1,0:T(8,128)(2,1)} %copy_bitcast_fusion.1), calls=%async_computation.4 | async-start | bytes 262144 | tf_op jit(solution)/shard_map/all_to_all | solution.py:27
  123.3 7.3 %all-to-all-done.4 = bf16[8,16,512]{2,1,0:T(8,128)(2,1)S(1)} async-done(((bf16[8,16,512]{2,1,0:T(8,128)(2,1)}), bf16[8,16,512]{2,1,0:T(8,128)(2,1)S(1)}, u32[]{:S(2)}, u32[]{:S(2)}) %all-to-all-start.4) | async-done | bytes 131104 | tf_op jit(solution)/shard_map/all_to_all | solution.py:27
  130.6 0.8 fusion
  (57 shorter events, 8.0 us)
Async XLA Ops:
  2.3 21.2 %all-to-all-start = ((bf16[8,32,640]{2,1,0:T(8,128)(2,1)}), bf16[8,32,640]{2,1,0:T(8,128)(2,1)}, u32[]{:S(2)}, u32[]{:S(2)}) async-start(bf16[8,32,640]{2,1,0:T(8,128)(2,1)} %broadcast_in_dim.6), calls=%async_computation | async-start | bytes 655360 | tf_op jit(solution)/shard_map/all_to_all | solution.py:27
  13.5 25.6 %copy-start.3 = (bf16[512,2048]{1,0:T(8,128)(2,1)S(1)}, bf16[512,2048]{1,0:T(8,128)(2,1)}, u32[]{:S(2)}) copy-start(bf16[512,2048]{1,0:T(8,128)(2,1)} %out_w_ref.1) | copy-start | bytes 6291460
  13.5 25.6 %copy-start.4 = (bf16[32,2048]{1,0:T(8,128)(2,1)S(1)}, bf16[32,2048]{1,0:T(8,128)(2,1)}, u32[]{:S(2)}) copy-start(bf16[32,2048]{1,0:T(8,128)(2,1)} %tokens_ref.1) | copy-start | bytes 393220
  13.5 25.6 %copy-start.5 = (f32[32,8,1024]{2,1,0:T(8,128)S(1)}, f32[32,8,1024]{2,1,0:T(8,128)}, u32[]{:S(2)}) copy-start(f32[32,8,1024]{2,1,0:T(8,128)} %cum_ref.1) | copy-start | bytes 3145732
  13.5 25.6 %copy-start.6 = (bf16[2048,8]{0,1:T(8,128)(2,1)S(1)}, bf16[2048,8]{0,1:T(8,128)(2,1)}, u32[]{:S(2)}) copy-start(bf16[2048,8]{0,1:T(8,128)(2,1)} %param.24) | copy-start | bytes 98308
  13.5 25.6 %copy-start.7 = (f32[2048]{0:T(1024)S(1)}, f32[2048]{0:T(1024)}, u32[]{:S(2)}) copy-start(f32[2048]{0:T(1024)} %param.20) | copy-start | bytes 24580
  13.5 25.6 %copy-start.10 = (f32[8]{0:T(128)S(1)}, f32[8]{0:T(128)}, u32[]{:S(2)}) copy-start(f32[8]{0:T(128)} %param.25) | copy-start | bytes 100
  13.5 25.6 %copy-start.11 = (s32[32]{0:T(128)S(1)}, s32[32]{0:T(128)}, u32[]{:S(2)}) copy-start(s32[32]{0:T(128)} %length_ref.1) | copy-start | bytes 388
  15.2 14.1 %collective-permute-start = (bf16[32,512]{1,0:T(8,128)(2,1)S(1)}, bf16[32,512]{1,0:T(8,128)(2,1)S(1)}, u32[]{:S(2)}, u32[]{:S(2)}) collective-permute-start(bf16[32,512]{1,0:T(8,128)(2,1)S(1)} %pad_maximum_fusion.2), channel_id=1, source_target_pairs={{0,8},{8,16},{16,24},{24,0},{1,9},{9,17},{17,25},{25,1},{2,10},{10... | collective-permute-start | bytes 98312 | tf_op jit(solution)/shard_map/ppermute | solution.py:23
  23.5 7.7 %collective-permute-start.3 = (bf16[8,32,640]{2,1,0:T(8,128)(2,1)}, bf16[8,32,640]{2,1,0:T(8,128)(2,1)S(1)}, u32[]{:S(2)}, u32[]{:S(2)}) collective-permute-start(bf16[8,32,640]{2,1,0:T(8,128)(2,1)} %all-to-all-done), channel_id=1, source_target_pairs={{0,4},{4,0},{1,5},{5,1},{2,6},{6,2},{3,7},{7,3},{8,12},{12,8},{9,1... | collective-permute-start | bytes 983048 | tf_op jit(solution)/shard_map/ppermute | solution.py:23
  25.6 4.3 %collective-permute-start.1 = (bf16[32,512]{1,0:T(8,128)(2,1)S(1)}, bf16[32,512]{1,0:T(8,128)(2,1)S(1)}, u32[]{:S(2)}, u32[]{:S(2)}) collective-permute-start(bf16[32,512]{1,0:T(8,128)(2,1)S(1)} %pad_maximum_fusion.3), channel_id=1, source_target_pairs={{0,16},{8,24},{16,0},{24,8},{1,17},{9,25},{17,1},{25,9},{2,18},{10... | collective-permute-start | bytes 98312 | tf_op jit(solution)/shard_map/ppermute | solution.py:23
  28.4 2.8 %collective-permute-start.2 = (bf16[32,512]{1,0:T(8,128)(2,1)S(1)}, bf16[32,512]{1,0:T(8,128)(2,1)S(1)}, u32[]{:S(2)}, u32[]{:S(2)}) collective-permute-start(bf16[32,512]{1,0:T(8,128)(2,1)S(1)} %pad_maximum_fusion.4), channel_id=1, source_target_pairs={{0,24},{8,0},{16,8},{24,16},{1,25},{9,1},{17,9},{25,17},{2,26},{10... | collective-permute-start | bytes 98312 | tf_op jit(solution)/shard_map/ppermute | solution.py:23
  32.6 4.1 %collective-permute-start.6 = (bf16[32,640]{1,0:T(8,128)(2,1)S(1)}, bf16[32,640]{1,0:T(8,128)(2,1)S(1)}, u32[]{:S(2)}, u32[]{:S(2)}) collective-permute-start(bf16[32,640]{1,0:T(8,128)(2,1)S(1)} %get-tuple-element.30), channel_id=1, source_target_pairs={{0,8},{8,16},{16,24},{24,0},{1,9},{9,17},{17,25},{25,1},{2,10},{10... | collective-permute-start | bytes 122888 | tf_op jit(solution)/shard_map/ppermute | solution.py:23
  33.5 4.4 %collective-permute-start.5 = (bf16[32,640]{1,0:T(8,128)(2,1)S(1)}, bf16[32,640]{1,0:T(8,128)(2,1)S(1)}, u32[]{:S(2)}, u32[]{:S(2)}) collective-permute-start(bf16[32,640]{1,0:T(8,128)(2,1)S(1)} %get-tuple-element.31), channel_id=1, source_target_pairs={{0,16},{8,24},{16,0},{24,8},{1,17},{9,25},{17,1},{25,9},{2,18},{10... | collective-permute-start | bytes 122888 | tf_op jit(solution)/shard_map/ppermute | solution.py:23
  35.9 3.1 %collective-permute-start.4 = (bf16[32,640]{1,0:T(8,128)(2,1)S(1)}, bf16[32,640]{1,0:T(8,128)(2,1)S(1)}, u32[]{:S(2)}, u32[]{:S(2)}) collective-permute-start(bf16[32,640]{1,0:T(8,128)(2,1)S(1)} %get-tuple-element.32), channel_id=1, source_target_pairs={{0,24},{8,0},{16,8},{24,16},{1,25},{9,1},{17,9},{25,17},{2,26},{10... | collective-permute-start | bytes 122888 | tf_op jit(solution)/shard_map/ppermute | solution.py:23
  39.1 16.6 %copy-start.8 = (s32[32,2]{0,1:T(2,128)S(1)}, s32[32,2]{0,1:T(2,128)}, u32[]{:S(2)}) copy-start(s32[32,2]{0,1:T(2,128)} %param.36) | copy-start | bytes 772
  39.1 16.6 %copy-start.9 = (f32[32,2]{0,1:T(2,128)S(1)}, f32[32,2]{0,1:T(2,128)}, u32[]{:S(2)}) copy-start(f32[32,2]{0,1:T(2,128)} %param.37) | copy-start | bytes 772
  39.1 21.7 %copy-start.12 = (f32[2048]{0:T(1024)S(1)}, f32[2048]{0:T(1024)}, u32[]{:S(2)}) copy-start(f32[2048]{0:T(1024)} %param.31) | copy-start | bytes 24580
  51.1 6.1 %collective-permute-start.9 = (bf16[32,2048]{1,0:T(8,128)(2,1)S(1)}, bf16[32,2048]{1,0:T(8,128)(2,1)S(1)}, u32[]{:S(2)}, u32[]{:S(2)}) collective-permute-start(bf16[32,2048]{1,0:T(8,128)(2,1)S(1)} %get-tuple-element.10), channel_id=1, source_target_pairs={{0,3},{1,0},{2,1},{3,2},{4,7},{5,4},{6,5},{7,6},{8,11},{9,8},{10,9... | collective-permute-start | bytes 393224 | tf_op jit(solution)/shard_map/ppermute | solution.py:23
  53.9 5.4 %collective-permute-start.8 = (bf16[32,2048]{1,0:T(8,128)(2,1)S(1)}, bf16[32,2048]{1,0:T(8,128)(2,1)S(1)}, u32[]{:S(2)}, u32[]{:S(2)}) collective-permute-start(bf16[32,2048]{1,0:T(8,128)(2,1)S(1)} %get-tuple-element.10), channel_id=1, source_target_pairs={{0,2},{1,3},{2,0},{3,1},{4,6},{5,7},{6,4},{7,5},{8,10},{9,11},{10,... | collective-permute-start | bytes 393224 | tf_op jit(solution)/shard_map/ppermute | solution.py:23
  54.2 6.4 %collective-permute-start.7 = (bf16[32,2048]{1,0:T(8,128)(2,1)S(1)}, bf16[32,2048]{1,0:T(8,128)(2,1)S(1)}, u32[]{:S(2)}, u32[]{:S(2)}) collective-permute-start(bf16[32,2048]{1,0:T(8,128)(2,1)S(1)} %get-tuple-element.10), channel_id=1, source_target_pairs={{0,1},{1,2},{2,3},{3,0},{4,5},{5,6},{6,7},{7,4},{8,9},{9,10},{10,1... | collective-permute-start | bytes 393224 | tf_op jit(solution)/shard_map/ppermute | solution.py:23
  61.0 34.2 %copy-start = (bf16[2048,256]{1,0:T(8,128)(2,1)S(1)}, bf16[2048,256]{1,0:T(8,128)(2,1)}, u32[]{:S(2)}) copy-start(bf16[2048,256]{1,0:T(8,128)(2,1)} %gate_ref.3) | copy-start | bytes 3145732
  61.0 34.2 %copy-start.1 = (bf16[2048,256]{1,0:T(8,128)(2,1)S(1)}, bf16[2048,256]{1,0:T(8,128)(2,1)}, u32[]{:S(2)}) copy-start(bf16[2048,256]{1,0:T(8,128)(2,1)} %up_ref.3) | copy-start | bytes 3145732
  61.1 34.2 %copy-start.2 = (bf16[256,2048]{1,0:T(8,128)(2,1)S(1)}, bf16[256,2048]{1,0:T(8,128)(2,1)}, u32[]{:S(2)}) copy-start(bf16[256,2048]{1,0:T(8,128)(2,1)} %down_ref.3) | copy-start | bytes 3145732
  86.6 8.6 %collective-permute-start.10 = (bf16[16,64,512]{2,1,0:T(8,128)(2,1)S(1)}, bf16[16,64,512]{2,1,0:T(8,128)(2,1)S(1)}, u32[]{:S(2)}, u32[]{:S(2)}) collective-permute-start(bf16[16,64,512]{2,1,0:T(8,128)(2,1)S(1)} %all_to_all.26.rows_ref), channel_id=1, source_target_pairs={{0,4},{4,0},{1,5},{5,1},{2,6},{6,2},{3,7},{7,3},{8,12},{12,8},{9,1... | collective-permute-start | bytes 3145736 | tf_op jit(solution)/shard_map/ppermute | solution.py:23
  96.4 2.7 %collective-permute-start.11 = (bf16[16,64,512]{2,1,0:T(8,128)(2,1)S(1)}, bf16[16,64,512]{2,1,0:T(8,128)(2,1)S(1)}, u32[]{:S(2)}, u32[]{:S(2)}) collective-permute-start(bf16[16,64,512]{2,1,0:T(8,128)(2,1)S(1)} %shard_map.213), channel_id=1, source_target_pairs={{0,4},{4,0},{1,5},{5,1},{2,6},{6,2},{3,7},{7,3},{8,12},{12,8},{9,1... | collective-permute-start | bytes 3145736 | tf_op jit(solution)/shard_map/ppermute | solution.py:23
  119.3 11.3 %all-to-all-start.4 = ((bf16[8,16,512]{2,1,0:T(8,128)(2,1)}), bf16[8,16,512]{2,1,0:T(8,128)(2,1)S(1)}, u32[]{:S(2)}, u32[]{:S(2)}) async-start(bf16[8,16,512]{2,1,0:T(8,128)(2,1)} %copy_bitcast_fusion.1), calls=%async_computation.4 | async-start | bytes 262144 | tf_op jit(solution)/shard_map/all_to_all | solution.py:27
where the time goes:
time: 133 us; the launch traced here: 131 us
  blocking collectives  44.2 us (33%)
  starting transfers between devices  33.7 us (25%)
  waiting for transfers between devices  27.2 us (20%)
  Pallas kernels  14.2 us (11%)
  local copies, waits for them, and re-layouts  5.89 us (4%)
  other arithmetic  2.74 us (2%)
  matrix products  2.42 us (2%)
    all_to_all x3, blocking collectives, exchange(): return lax.all_to_all(blocks, axis, split_axis=0, concat_axis=0, tiled=True)  44.2 us
    ppermute x12, starting transfers between devices, shifted(): return lax.ppermute(value, axis, [(i, (i + step) % n) for i in range(n)])  21.3 us
    all_to_all x2, waiting for transfers between devices, exchange(): return lax.all_to_all(blocks, axis, split_axis=0, concat_axis=0, tiled=True)  14.3 us
    ppermute x12, waiting for transfers between devices, shifted(): return lax.ppermute(value, axis, [(i, (i + step) % n) for i in range(n)])  12.9 us
    all_to_all x2, starting transfers between devices, exchange(): return lax.all_to_all(blocks, axis, split_axis=0, concat_axis=0, tiled=True)  12.4 us
    pallas_call x1, Pallas kernels, attend(): pl.pallas_call(functools.partial(attend_kernel, together), out_shape=(jax...  11.9 us
  transfers between devices with their start and end apart: 14, of which 12 were waited for; matrix products, arithmetic and copies ran while one was open for 4% of the time, Pallas kernels for 1%

commit v1 on v0

--- a/solution.py
+++ b/solution.py
@@ -66,60 +66,58 @@
 
 def attend_kernel(
     together,
-    tokens_ref,
-    gain_ref,
-    forget_ref,
-    bias_ref,
+    parts,
     own_ref,
     pieces_refs,
+    scale_ref,
+    gate_ref,
+    length_ref,
     cum_ref,
-    length_ref,
     keys_ref,
     values_ref,
     out_w_ref,
     mix_ref,
     key_ref,
     value_ref,
-    gate_ref,
     q_s,
     own_s,
-    gate_s,
     weight_s,
     heads_s,
+    past_s,
+    cum_s,
     keys_s,
     values_s,
+    out_w_s,
     sems,
 ):
-    rows = tokens_ref.shape[0]
-    _, head_dim, span_len = keys_ref.shape
-    _, group, _ = q_s.shape
+    rows, group, head_dim = q_s.shape
+    span_len = keys_ref.shape[2]
     cols = group * head_dim
     scale = HEAD_DIM ** (-0.5)
-    copies = []
-    for step in range(rows // together):
-        some = pl.ds(step * together, together)
-        copies.append(
-            (
-                pltpu.make_async_copy(keys_ref.at[some], keys_s.at[some], sems.at[0, step]),
-                pltpu.make_async_copy(values_ref.at[some], values_s.at[some], sems.at[1, step]),
-            )
-        )
-        for copy in copies[step]:
-            copy.start()
-
-    tokens = tokens_ref[...].astype(F32)
-    scale_attn = lax.rsqrt(jnp.mean(tokens * tokens, axis=1, keepdims=True) + EPSILON)
-    normed = (tokens * scale_attn * gain_ref[...]).astype(BF16)
-    logits = lax.dot_general(
-        normed, forget_ref[...], (((1,), (1,)), ((), ())), preferred_element_type=F32
-    )
-    logits = logits + bias_ref[...]
-    gate = jnp.minimum(logits, 0.0) - jnp.log1p(jnp.exp(-jnp.abs(logits)))
-    gate_ref[...] = gate
+    share = rows // parts
+    halves = [pl.ds(p * share, share) for p in range(parts)]
+
+    def copies(number, source, target):
+        return [
+            pltpu.make_async_copy(source.at[h], target.at[h], sems.at[number, p])
+            for p, h in enumerate(halves)
+        ]
+
+    key_copies = copies(0, keys_ref, keys_s)
+    cum_copies = copies(1, cum_ref, cum_s)
+    value_copies = copies(2, values_ref, values_s)
+    out_w_copy = pltpu.make_async_copy(out_w_ref, out_w_s, sems.at[3, 0])
+    for p in range(parts):
+        cum_copies[p].start()
+        key_copies[p].start()
+    for copy in value_copies:
+        copy.start()
+    out_w_copy.start()
+
     projected = own_ref[...]
     for ref in pieces_refs:
         projected = projected + ref[...].astype(F32)
-    projected = projected * scale_attn
+    projected = projected * scale_ref[...]
     new_key = projected[:, cols : cols + head_dim].astype(BF16)
     new_value = projected[:, cols + head_dim : cols + 2 * head_dim].astype(BF16)
     key_ref[...] = new_key
@@ -143,69 +141,89 @@
     own_s[...] = (
         jnp.sum(by_head * new_key.astype(F32)[:, None, :], axis=2, keepdims=True) * scale
     )
-    same = lax.broadcasted_iota(jnp.int32, (rows, group, group), 1) == lax.broadcasted_iota(
-        jnp.int32, (rows, group, group), 2
-    )
-    gate_s[...] = jnp.sum(jnp.where(same, gate[:, None, :], 0.0), axis=2, keepdims=True)
     places = lax.broadcasted_iota(jnp.int32, (group, span_len), 1)
 
-    for step in range(rows // together):
-        for copy in copies[step]:
-            copy.wait()
-        for k in range(together):
-            b = step * together + k
-            length = length_ref[b]
-            scores = jnp.dot(q_s[b].astype(BF16), keys_s[b], preferred_element_type=F32) * scale
-            cum = cum_ref[b]
-            last = jnp.sum(jnp.where(places == length - 1, cum, 0.0), axis=1, keepdims=True)
-            past = jnp.where(places < length, scores + ((last + gate_s[b]) - cum), MASKED)
-            own = own_s[b]
-            peak = jnp.maximum(jnp.max(past, axis=1, keepdims=True), own)
-            past_exp = jnp.exp(past - peak)
-            own_exp = jnp.exp(own - peak)
-            total = jnp.sum(past_exp, axis=1, keepdims=True) + own_exp
-            weight = (past_exp / total).astype(BF16)
+    def weigh(some):
+        scores = [
+            jnp.dot(q_s[b].astype(BF16), keys_s[b], preferred_element_type=F32) * scale
+            for b in some
+        ]
+        lengths = [length_ref[b] for b in some]
+        cums = [cum_s[b] for b in some]
+        lasts = [
+            jnp.sum(jnp.where(places == n - 1, cum, 0.0), axis=1, keepdims=True)
+            for n, cum in zip(lengths, cums)
+        ]
+        pasts = [
+            jnp.where(places < n, score + ((last + gate_ref[b]) - cum), MASKED)
+            for b, n, score, last, cum in zip(some, lengths, scores, lasts, cums)
+        ]
+        owns = [own_s[b] for b in some]
+        peaks = [
+            jnp.maximum(jnp.max(past, axis=1, keepdims=True), own)
+            for past, own in zip(pasts, owns)
+        ]
+        past_exps = [jnp.exp(past - peak) for past, peak in zip(pasts, peaks)]
+        own_exps = [jnp.exp(own - peak) for own, peak in zip(owns, peaks)]
+        totals = [
+            jnp.sum(past_exp, axis=1, keepdims=True) + own_exp
+            for past_exp, own_exp in zip(past_exps, own_exps)
+        ]
+        for b, past_exp, own_exp, total in zip(some, past_exps, own_exps, totals):
             weight_s[b] = own_exp / total
-            heads_s[b] = lax.dot_general(
-                weight, values_s[b], (((1,), (1,)), ((), ())), preferred_element_type=F32
+            past_s[b] = (past_exp / total).astype(BF16)
+
+    def mix(some):
+        mixed = [
+            lax.dot_general(
+                past_s[b], values_s[b], (((1,), (1,)), ((), ())), preferred_element_type=F32
             )
+            for b in some
+        ]
+        for b, one in zip(some, mixed):
+            heads_s[b] = one
+
+    for p in range(parts):
+        cum_copies[p].wait()
+        key_copies[p].wait()
+        for first in range(p * share, (p + 1) * share, together):
+            weigh(range(first, first + together))
+    for p in range(parts):
+        value_copies[p].wait()
+        mix(range(p * share, (p + 1) * share))
     own_weight = weight_s[...].astype(BF16).astype(F32)
     heads = heads_s[...] + own_weight * new_value.astype(F32)[:, None, :]
     heads = heads.reshape(rows * group, head_dim).astype(BF16)
     wide = lax.dot_general(heads, fold, (((1,), (1,)), ((), ())), preferred_element_type=F32)
     wide = jnp.where(on_head, wide.reshape(rows, group, cols), 0.0)
     heads_out = jnp.sum(wide, axis=1).astype(BF16)
-    mix_ref[...] = jnp.dot(heads_out, out_w_ref[...], preferred_element_type=F32).astype(BF16)
-
-
-def attend(tokens, gain, forget, bias, own, pieces, cum, lengths, keys, values, out_w):
-    rows, width = tokens.shape
-    group, head_dim = cum.shape[1], keys.shape[1]
+    out_w_copy.wait()
+    mix_ref[...] = jnp.dot(heads_out, out_w_s[...], preferred_element_type=F32).astype(BF16)
+
+
+def attend(own, pieces, scale, gate, lengths, cum, keys, values, out_w):
+    rows, group, _ = cum.shape
+    head_dim, width = keys.shape[1], out_w.shape[1]
     in_vmem = pl.BlockSpec(memory_space=pltpu.VMEM)
-    in_smem = pl.BlockSpec(memory_space=pltpu.SMEM)
-    in_hbm = pl.BlockSpec(memory_space=pltpu.HBM)
+    from_hbm = pl.BlockSpec(memory_space=pltpu.HBM)
     one = jax.ShapeDtypeStruct((rows, head_dim), BF16)
-    together = 8
+    together, parts = 8, 2
     return pl.pallas_call(
-        functools.partial(attend_kernel, together),
-        out_shape=(
-            jax.ShapeDtypeStruct((rows, width), BF16),
-            one,
-            one,
-            jax.ShapeDtypeStruct((rows, group), F32),
-        ),
-        in_specs=[in_vmem] * 5
-        + [[in_vmem] * len(pieces), in_vmem, in_smem, in_hbm, in_hbm, in_vmem],
-        out_specs=(in_vmem,) * 4,
+        functools.partial(attend_kernel, together, parts),
+        out_shape=(jax.ShapeDtypeStruct((rows, width), BF16), one, one),
+        in_specs=[in_vmem, [in_vmem] * len(pieces)] + [in_vmem] * 3 + [from_hbm] * 4,
+        out_specs=(in_vmem,) * 3,
         scratch_shapes=[
             pltpu.VMEM((rows, group, head_dim), F32),
             pltpu.VMEM((rows, group, 1), F32),
             pltpu.VMEM((rows, group, 1), F32),
-            pltpu.VMEM((rows, group, 1), F32),
             pltpu.VMEM((rows, group, head_dim), F32),
+            pltpu.VMEM(cum.shape, BF16),
+            pltpu.VMEM(cum.shape, F32),
             pltpu.VMEM(keys.shape, BF16),
             pltpu.VMEM(values.shape, BF16),
-            pltpu.SemaphoreType.DMA((2, rows // together)),
+            pltpu.VMEM(out_w.shape, BF16),
+            pltpu.SemaphoreType.DMA((4, parts)),
         ],
         compiler_params=pltpu.CompilerParams(vmem_limit_bytes=24 * 2**20),
         cost_estimate=pl.CostEstimate(
@@ -213,11 +231,129 @@
             bytes_accessed=4 * keys.size + 4 * cum.size + 2 * out_w.size,
             transcendentals=cum.size,
         ),
-    )(tokens, gain, forget, bias, own, pieces, cum, lengths, keys, values, out_w)
-
-
-def slots_kernel(routes_ref, weights_ref, selector_ref, weighing_ref):
-    top, rows = routes_ref.shape
+    )(own, pieces, scale, gate, lengths, *in_hbm(cum, keys, values, out_w))
+
+
+def cut_kernel(nz, nx, *refs):
+    outs, cut_s = refs[2 : 2 + nx], refs[2 + nx]
+    tokens_ref, gain_ref = fetched(refs[:2], refs[3 + nx : -1], refs[-1])
+    _, width = tokens_ref.shape
+    chunk = width // (nz * nx)
+    scaled = (tokens_ref[...].astype(F32) * gain_ref[...])
+    for x in range(nx):
+        cut_s[x] = jnp.concatenate(
+            [scaled[:, (z * nx + x) * chunk : (z * nx + x + 1) * chunk] for z in range(nz)], axis=1
+        )
+    here = lax.axis_index("x")
+    for s in range(nx):
+        outs[s][...] = cut_s[lax.rem(here + s, nx)].astype(BF16)
+
+
+def cut_tokens(tokens, gain, nz, nx):
+    rows, width = tokens.shape
+    in_vmem = pl.BlockSpec(memory_space=pltpu.VMEM)
+    return pl.pallas_call(
+        functools.partial(cut_kernel, nz, nx),
+        out_shape=[jax.ShapeDtypeStruct((rows, width // nx), BF16)] * nx,
+        in_specs=[pl.BlockSpec(memory_space=pltpu.HBM)] * 2,
+        out_specs=[in_vmem] * nx,
+        scratch_shapes=[pltpu.VMEM((nx, rows, width // nx), F32)] + places_for((tokens, gain)),
+        compiler_params=pltpu.CompilerParams(vmem_limit_bytes=4 * 2**20),
+    )(*in_hbm(tokens, gain))
+
+
+def multiply_kernel(count, *refs):
+    token_refs, (same_ref, other_ref), outs = refs[:count], refs[count : count + 2], refs[count + 2 :]
+    first = lax.axis_index("c") == 0
+    same, other = same_ref[...], other_ref[...]
+    weights = jnp.concatenate(
+        (jnp.where(first, same, other), jnp.where(first, other, same)), axis=1
+    )
+    weights = weights.reshape(-1, weights.shape[-1])
+    tokens = jnp.concatenate([ref[...] for ref in token_refs], axis=0)
+    product = jnp.dot(tokens, weights, preferred_element_type=F32)
+    rows = token_refs[0].shape[0]
+    for s, out in enumerate(outs):
+        out[...] = product[s * rows : (s + 1) * rows].astype(out.dtype)
+
+
+def multiply(pieces, same, other):
+    rows = pieces[0].shape[0]
+    cols = same.shape[2]
+    in_vmem = pl.BlockSpec(memory_space=pltpu.VMEM)
+    kinds = [F32] + [BF16] * (len(pieces) - 1)
+    return pl.pallas_call(
+        functools.partial(multiply_kernel, len(pieces)),
+        out_shape=[jax.ShapeDtypeStruct((rows, cols), kind) for kind in kinds],
+        in_specs=[in_vmem] * (len(pieces) + 2),
+        out_specs=[in_vmem] * len(pieces),
+        compiler_params=pltpu.CompilerParams(vmem_limit_bytes=8 * 2**20),
+        cost_estimate=pl.CostEstimate(
+            flops=4 * rows * len(pieces) * same.size,
+            bytes_accessed=4 * same.size,
+            transcendentals=0,
+        ),
+    )(*pieces, same, other)
+
+
+def fetched(sources, targets, sems):
+    copies = [
+        pltpu.make_async_copy(source, target, sems.at[k])
+        for k, (source, target) in enumerate(zip(sources, targets))
+    ]
+    for copy in copies:
+        copy.start()
+    for copy in copies:
+        copy.wait()
+    return targets
+
+
+def in_hbm(*arrays):
+    return [pltpu.with_memory_space_constraint(array, pltpu.HBM) for array in arrays]
+
+
+def places_for(arrays):
+    return [pltpu.VMEM(array.shape, array.dtype) for array in arrays] + [
+        pltpu.SemaphoreType.DMA((len(arrays),))
+    ]
+
+
+def early_kernel(count, *refs):
+    scale_ref, log_gate_ref, gate_ref, long_ref, selector_ref, weighing_ref = refs[count : count + 6]
+    (
+        tokens_ref,
+        gain_ref,
+        forget_ref,
+        bias_ref,
+        length_ref,
+        routes_ref,
+        weights_ref,
+    ) = fetched(refs[:count], refs[count + 6 : -1], refs[-1])
+
+    tokens = tokens_ref[...].astype(F32)
+    rows = tokens.shape[0]
+    group = forget_ref.shape[0]
+    scale = lax.rsqrt(jnp.mean(tokens * tokens, axis=1, keepdims=True) + EPSILON)
+    scale_ref[...] = scale
+    normed = (tokens * scale * gain_ref[...]).astype(BF16)
+    logits = lax.dot_general(
+        normed, forget_ref[...], (((1,), (1,)), ((), ())), preferred_element_type=F32
+    )
+    logits = logits + bias_ref[...]
+    gate = jnp.minimum(logits, 0.0) - jnp.log1p(jnp.exp(-jnp.abs(logits)))
+    log_gate_ref[...] = gate
+    same = lax.broadcasted_iota(jnp.int32, (rows, group, group), 1) == lax.broadcasted_iota(
+        jnp.int32, (rows, group, group), 2
+    )
+    gate_ref[...] = jnp.sum(jnp.where(same, gate[:, None, :], 0.0), axis=2, keepdims=True)
+    mine = lax.broadcasted_iota(jnp.int32, (rows, rows), 0) == lax.broadcasted_iota(
+        jnp.int32, (rows, rows), 1
+    )
+    lengths = jnp.where(mine, length_ref[...].astype(F32), 0.0)
+    lengths = jnp.sum(lengths, axis=1, keepdims=True)
+    long_ref[...] = jnp.broadcast_to(lengths[:, None, :], long_ref.shape).astype(jnp.int32)
+
+    top = routes_ref.shape[0]
     named = [routes_ref[pl.ds(k, 1), :] for k in range(top)]
     experts = lax.broadcasted_iota(jnp.int32, (EXPERTS, rows), 0)
     hits = [jnp.where(experts == one, 1.0, 0.0) for one in named]
@@ -240,16 +376,26 @@
     weighing_ref[...] = weighed
 
 
-def slots(routes, weights):
+def early(*arrays):
     in_vmem = pl.BlockSpec(memory_space=pltpu.VMEM)
-    shape = (EXPERTS * CAP, routes.shape[1])
+    tokens, _, forget, *_ = arrays
+    rows, group = tokens.shape[0], forget.shape[0]
+    slots = EXPERTS * CAP
     return pl.pallas_call(
-        slots_kernel,
-        out_shape=(jax.ShapeDtypeStruct(shape, BF16), jax.ShapeDtypeStruct(shape, F32)),
-        in_specs=[in_vmem] * 2,
-        out_specs=(in_vmem,) * 2,
-        compiler_params=pltpu.CompilerParams(vmem_limit_bytes=4 * 2**20),
-    )(routes, weights)
+        functools.partial(early_kernel, len(arrays)),
+        out_shape=(
+            jax.ShapeDtypeStruct((rows, 1), F32),
+            jax.ShapeDtypeStruct((rows, group), F32),
+            jax.ShapeDtypeStruct((rows, group, 1), F32),
+            jax.ShapeDtypeStruct((rows, group, 1), jnp.int32),
+            jax.ShapeDtypeStruct((slots, rows), BF16),
+            jax.ShapeDtypeStruct((slots, rows), F32),
+        ),
+        in_specs=[pl.BlockSpec(memory_space=pltpu.HBM)] * len(arrays),
+        out_specs=(in_vmem,) * 6,
+        scratch_shapes=places_for(arrays),
+        compiler_params=pltpu.CompilerParams(vmem_limit_bytes=6 * 2**20),
+    )(*in_hbm(*arrays))
 
 
 def layer(
@@ -273,53 +419,37 @@
     routes,
     route_weights,
 ):
-    rows, width = tokens.shape
-    nz, nx, nc, ny = (lax.axis_size(a) for a in ("z", "x", "c", "y"))
-    ix, ic, iy = lax.axis_index("x"), lax.axis_index("c"), lax.axis_index("y")
-
-    selector, weighing = slots(routes.T, route_weights.T)
-
-    weights = jnp.concatenate((w_query, w_key, w_value), axis=1)
-    cols = weights.shape[1]
-    same_core = exchange(jnp.broadcast_to(weights, (nz, *weights.shape)), "z")
-    other_core = shifted(same_core, "c", 1)
-    deep = width // (nx * nc)
-    scaled = (tokens.astype(F32) * norm_gain_attn).astype(BF16)
-    scaled = scaled.reshape(rows, nz, nx, nc, width // (nz * nx * nc)).transpose(2, 3, 0, 1, 4)
-    scaled = scaled.reshape(nx, nc, rows, deep)
-    mine = [
-        jnp.concatenate(
-            [
-                lax.dynamic_slice(
-                    scaled, ((ix + s) % nx, (ic + k) % nc, 0, 0), (1, 1, rows, deep)
-                )[0, 0]
-                for k in range(nc)
-            ],
-            axis=1,
-        )
-        for s in range(nx)
-    ]
-    moved = [shifted(mine[s], "x", s) for s in range(1, nx)]
-    part_tokens = jnp.concatenate([mine[0]] + moved, axis=0)
-    partial = jnp.dot(
-        part_tokens[:, :deep], same_core.reshape(deep, cols), preferred_element_type=F32
-    ) + jnp.dot(part_tokens[:, deep:], other_core.reshape(deep, cols), preferred_element_type=F32)
-    pieces = [
-        shifted(partial[s * rows : (s + 1) * rows].astype(BF16), "x", nx - s)
-        for s in range(1, nx)
-    ]
-
-    partial_mix, new_keys, new_values, new_log_gate = attend(
+    _, width = tokens.shape
+    nz, nx, _, ny = (lax.axis_size(a) for a in ("z", "x", "c", "y"))
+    iy = lax.axis_index("y")
+
+    scale_attn, new_log_gate, gate, long, selector, weighing = early(
         tokens,
         norm_gain_attn.reshape(1, width),
         w_forget.T,
         forget_bias.reshape(1, -1),
-        partial[:rows],
+        lengths.reshape(1, -1),
+        routes.T,
+        route_weights.T,
+    )
+
+    weights = jnp.concatenate((w_query, w_key, w_value), axis=1)
+    same_core = exchange(jnp.broadcast_to(weights, (nz, *weights.shape)), "z")
+    other_core = shifted(same_core, "c", 1)
+    mine = cut_tokens(tokens, norm_gain_attn.reshape(1, width), nz, nx)
+    moved = [shifted(mine[s], "x", s) for s in range(1, nx)]
+    own_partial, *partials = multiply([mine[0]] + moved, same_core, other_core)
+    pieces = [shifted(partials[s - 1], "x", nx - s) for s in range(1, nx)]
+
+    partial_mix, new_keys, new_values = attend(
+        own_partial,
         pieces,
+        scale_attn,
+        gate,
+        long,
         cache_logcum,
-        lengths,
-        pltpu.with_memory_space_constraint(cache_keys, pltpu.HBM),
-        pltpu.with_memory_space_constraint(cache_values, pltpu.HBM),
+        cache_keys,
+        cache_values,
         w_out,
     )
 

time: 133 us -> 127 us (0.955)
  blocking collectives: 44.2 us -> 64.6 us
  starting transfers between devices: 33.7 us -> 25.2 us
  waiting for transfers between devices: 27.2 us -> 19.8 us
  local copies, waits for them, and re-layouts: 5.89 us -> 2.24 us
  Pallas kernels: 14.2 us -> 10.6 us
  matrix products: 2.42 us -> 1.03 us
    all_to_all x3 -> x4, blocking collectives: 44.2 us -> 64.6 us  [exchange(): return lax.all_to_all(blocks, axis, split_axis=0, concat_axis=0, tiled=True)]
    all_to_all x2 -> x1, starting transfers between devices: 12.4 us -> 3.37 us  [exchange(): return lax.all_to_all(blocks, axis, split_axis=0, concat_axis=0, tiled=True)]
    all_to_all x2 -> x1, waiting for transfers between devices: 14.3 us -> 7.28 us  [exchange(): return lax.all_to_all(blocks, axis, split_axis=0, concat_axis=0, tiled=True)]
    pallas_call x2 -> x4, Pallas kernels: 12.1 us -> 8.45 us  [the longest x1 5.71 us: attend(): pl.pallas_call(functools.partial(attend_kernel, together, parts), out_sha...]
    reshape x3 -> x0, local copies, waits for them, and re-layouts: 2.82 us -> none  [the longest x1 1.59 us: layer(): scaled = scaled.reshape(nx, nc, rows, deep)]
    dot_general x2 -> x0, matrix products: 1.39 us -> none  [the longest x1 1.19 us: layer(): jnp.dot(part_tokens[:, :deep], same_core.reshape(deep, cols), preferred_e...]
  transfers between devices with their start and end apart: 14 -> 13, of which waited for: 12 -> 9; matrix products, arithmetic and copies ran while one was open for 4% -> 1% of each run, Pallas kernels for 1% -> 3%
where the time goes in v1:
time: 127 us; the launch traced here: 126 us
  blocking collectives  64.6 us (51%)
  starting transfers between devices  25.2 us (20%)
  waiting for transfers between devices  19.8 us (16%)
  Pallas kernels  10.6 us (8%)
  local copies, waits for them, and re-layouts  2.24 us (2%)
  other arithmetic  1.77 us (1%)
    all_to_all x4, blocking collectives, exchange(): return lax.all_to_all(blocks, axis, split_axis=0, concat_axis=0, tiled=True)  64.6 us
    ppermute x12, starting transfers between devices, shifted(): return lax.ppermute(value, axis, [(i, (i + step) % n) for i in range(n)])  21.9 us
    ppermute x12, waiting for transfers between devices, shifted(): return lax.ppermute(value, axis, [(i, (i + step) % n) for i in range(n)])  12.6 us
    all_to_all x1, waiting for transfers between devices, exchange(): return lax.all_to_all(blocks, axis, split_axis=0, concat_axis=0, tiled=True)  7.28 us
    pallas_call x1, Pallas kernels, attend(): pl.pallas_call(functools.partial(attend_kernel, together, parts), out_sha...  5.71 us
    all_to_all x1, starting transfers between devices, exchange(): return lax.all_to_all(blocks, axis, split_axis=0, concat_axis=0, tiled=True)  3.37 us
  transfers between devices with their start and end apart: 13, of which 9 were waited for; matrix products, arithmetic and copies ran while one was open for 1% of the time, Pallas kernels for 3%

profile of v1, /device:TPU:1, one launch (start us, length us, event | category | flops | bytes accessed | tf_op | source)
XLA Modules:
  0.0 126.1 jit_solution(7036835918953907519)
XLA Ops:
  0.6 0.9 pad_maximum_fusion
  1.5 20.6 %all_to_all.25.refs_4_ = bf16[8,32,640]{2,1,0:T(8,128)(2,1)S(1)} all-to-all(bf16[8,32,640]{2,1,0:T(8,128)(2,1)S(1)} %broadcast_in_dim.6), channel_id=1, replica_groups=mesh['z'=8,'x'=4,'c'=2,'y'=4] {'z'}, dimensions={0} | all-to-all | bytes 655360 | tf_op jit(solution)/shard_map/all_to_all | solution.py:27
  22.1 2.5 %collective-permute-start.3 = (bf16[8,32,640]{2,1,0:T(8,128)(2,1)S(1)}, bf16[8,32,640]{2,1,0:T(8,128)(2,1)S(1)}, u32[]{:S(2)}, u32[]{:S(2)}) collective-permute-start(bf16[8,32,640]{2,1,0:T(8,128)(2,1)S(1)} %all_to_all.25.refs_4_), channel_id=1, source_target_pairs={{0,4},{4,0},{1,5},{5,1},{2,6},{6,2},{3,7},{7,3},{8,12},{12,8},{9,1... | collective-permute-start | bytes 983048 | tf_op jit(solution)/shard_map/ppermute | solution.py:23
  24.6 1.1 shard_map.210
  25.7 1.3 %collective-permute-start = (bf16[32,512]{1,0:T(8,128)(2,1)S(1)}, bf16[32,512]{1,0:T(8,128)(2,1)S(1)}, u32[]{:S(2)}, u32[]{:S(2)}) collective-permute-start(bf16[32,512]{1,0:T(8,128)(2,1)S(1)} %get-tuple-element.22), channel_id=1, source_target_pairs={{0,8},{8,16},{16,24},{24,0},{1,9},{9,17},{17,25},{25,1},{2,10},{10... | collective-permute-start | bytes 98312 | tf_op jit(solution)/shard_map/ppermute | solution.py:23
  27.0 2.5 %collective-permute-start.1 = (bf16[32,512]{1,0:T(8,128)(2,1)S(1)}, bf16[32,512]{1,0:T(8,128)(2,1)S(1)}, u32[]{:S(2)}, u32[]{:S(2)}) collective-permute-start(bf16[32,512]{1,0:T(8,128)(2,1)S(1)} %get-tuple-element.23), channel_id=1, source_target_pairs={{0,16},{8,24},{16,0},{24,8},{1,17},{9,25},{17,1},{25,9},{2,18},{10... | collective-permute-start | bytes 98312 | tf_op jit(solution)/shard_map/ppermute | solution.py:23
  29.4 1.2 collective-permute-start.2
  30.6 1.0 collective-permute-done.1.refs_2_
  31.5 0.7 collective-permute-done.2.refs_3_
  32.6 2.4 %collective-permute-start.4 = (bf16[32,640]{1,0:T(8,128)(2,1)S(1)}, bf16[32,640]{1,0:T(8,128)(2,1)S(1)}, u32[]{:S(2)}, u32[]{:S(2)}) collective-permute-start(bf16[32,640]{1,0:T(8,128)(2,1)S(1)} %get-tuple-element.26), channel_id=1, source_target_pairs={{0,24},{8,0},{16,8},{24,16},{1,25},{9,1},{17,9},{25,17},{2,26},{10... | collective-permute-start | bytes 122888 | tf_op jit(solution)/shard_map/ppermute | solution.py:23
  34.9 0.7 collective-permute-start.6
  35.6 1.4 %shard_map.212 = (f32[32,1]{1,0:T(8,128)S(1)}, f32[32,8]{1,0:T(8,128)S(1)}, f32[32,8,1]{2,1,0:T(8,128)S(1)}, s32[32,8,1]{2,1,0:T(8,128)S(1)}, bf16[128,32]{1,0:T(8,128)(2,1)S(1)}, /*index=5*/f32[128,32]{1,0:T(8,128)S(1)}) custom-call(bf16[32,2048]{1,0:T(8,128)(2,1)} %refs_0_.3, f32[1,2048]{1,0:T(1,128)} %bitcast.30, bf16[8,2048]{1,0:T(8,128)(2,1)} %bitcast.31, ...), custom_call_target="tpu_custom_call" | custom-call | tf_op jit(solution)/shard_map/pallas_call | solution.py:384
  37.0 2.4 %collective-permute-done.5.pieces_refs_1_ = bf16[32,640]{1,0:T(8,128)(2,1)S(1)} collective-permute-done((bf16[32,640]{1,0:T(8,128)(2,1)S(1)}, bf16[32,640]{1,0:T(8,128)(2,1)S(1)}, u32[]{:S(2)}, u32[]{:S(2)}) %collective-permute-start.5) | collective-permute-done | bytes 40992 | tf_op jit(solution)/shard_map/ppermute | solution.py:23
  39.4 5.7 %shard_map.213 = (bf16[32,2048]{1,0:T(8,128)(2,1)S(1)}, bf16[32,64]{1,0:T(8,128)(2,1)}, bf16[32,64]{1,0:T(8,128)(2,1)}) custom-call(f32[32,640]{1,0:T(8,128)S(1)} %get-tuple-element.25.own_ref, bf16[32,640]{1,0:T(8,128)(2,1)S(1)} %collective-permute-done.4.pieces_refs_0_, bf16[32,640]{1,0:T(8,128)(2,1)S(1)} %collective-permute-done.5.pieces_refs_1_, ...), custom_call_target="tpu_custom_call" | custom-call | flops 134217728 | bytes 11534336 | tf_op jit(solution)/shard_map/pallas_call | solution.py:211
  45.1 2.8 %collective-permute-start.9 = (bf16[32,2048]{1,0:T(8,128)(2,1)S(1)}, bf16[32,2048]{1,0:T(8,128)(2,1)S(1)}, u32[]{:S(2)}, u32[]{:S(2)}) collective-permute-start(bf16[32,2048]{1,0:T(8,128)(2,1)S(1)} %get-tuple-element.32), channel_id=1, source_target_pairs={{0,3},{1,0},{2,1},{3,2},{4,7},{5,4},{6,5},{7,6},{8,11},{9,8},{10,9... | collective-permute-start | bytes 393224 | tf_op jit(solution)/shard_map/ppermute | solution.py:23
  48.3 0.7 collective-permute-start.7
  49.0 0.8 dynamic_slice.7
  49.8 1.5 %collective-permute-done.9 = bf16[32,2048]{1,0:T(8,128)(2,1)S(1)} collective-permute-done((bf16[32,2048]{1,0:T(8,128)(2,1)S(1)}, bf16[32,2048]{1,0:T(8,128)(2,1)S(1)}, u32[]{:S(2)}, u32[]{:S(2)}) %collective-permute-start.9) | collective-permute-done | bytes 131104 | tf_op jit(solution)/shard_map/ppermute | solution.py:23
  51.3 2.1 %collective-permute-done.8 = bf16[32,2048]{1,0:T(8,128)(2,1)S(1)} collective-permute-done((bf16[32,2048]{1,0:T(8,128)(2,1)S(1)}, bf16[32,2048]{1,0:T(8,128)(2,1)S(1)}, u32[]{:S(2)}, u32[]{:S(2)}) %collective-permute-start.8) | collective-permute-done | bytes 131104 | tf_op jit(solution)/shard_map/ppermute | solution.py:23
  53.4 1.3 %collective-permute-done.7 = bf16[32,2048]{1,0:T(8,128)(2,1)S(1)} collective-permute-done((bf16[32,2048]{1,0:T(8,128)(2,1)S(1)}, bf16[32,2048]{1,0:T(8,128)(2,1)S(1)}, u32[]{:S(2)}, u32[]{:S(2)}) %collective-permute-start.7) | collective-permute-done | bytes 131104 | tf_op jit(solution)/shard_map/ppermute | solution.py:23
  55.4 10.4 %all_to_all.26 = bf16[8,16,512]{2,1,0:T(8,128)(2,1)S(1)} all-to-all(bf16[8,16,512]{2,1,0:T(8,128)(2,1)S(1)} %bitcast.27), channel_id=1, replica_groups=mesh['z'=8,'x'=4,'c'=2,'y'=4] {'z'}, dimensions={0} | all-to-all | bytes 262144 | tf_op jit(solution)/shard_map/all_to_all | solution.py:27
  66.0 14.6 %all_to_all.27.rows_ref = bf16[16,64,512]{2,1,0:T(8,128)(2,1)S(1)} all-to-all(bf16[16,64,512]{2,1,0:T(8,128)(2,1)S(1)} %bitcast.26), channel_id=1, replica_groups=mesh['z'=8,'x'=4,'c'=2,'y'=4] {'x','y'}, dimensions={0} | all-to-all | bytes 2097152 | tf_op jit(solution)/shard_map/all_to_all | solution.py:27
  80.6 7.1 %collective-permute-start.10 = (bf16[16,64,512]{2,1,0:T(8,128)(2,1)S(1)}, bf16[16,64,512]{2,1,0:T(8,128)(2,1)S(1)}, u32[]{:S(2)}, u32[]{:S(2)}) collective-permute-start(bf16[16,64,512]{2,1,0:T(8,128)(2,1)S(1)} %all_to_all.27.rows_ref), channel_id=1, source_target_pairs={{0,4},{4,0},{1,5},{5,1},{2,6},{6,2},{3,7},{7,3},{8,12},{12,8},{9,1... | collective-permute-start | bytes 3145736 | tf_op jit(solution)/shard_map/ppermute | solution.py:23
  87.7 2.3 %collective-permute-done.10.rows_ref = bf16[16,64,512]{2,1,0:T(8,128)(2,1)S(1)} collective-permute-done((bf16[16,64,512]{2,1,0:T(8,128)(2,1)S(1)}, bf16[16,64,512]{2,1,0:T(8,128)(2,1)S(1)}, u32[]{:S(2)}, u32[]{:S(2)}) %collective-permute-start.10) | collective-permute-done | bytes 1048608 | tf_op jit(solution)/shard_map/ppermute | solution.py:23
  90.0 1.1 shard_map.215
  91.6 1.1 shard_map.214
  92.7 1.2 collective-permute-done.11
  94.2 19.0 %all_to_all.28 = bf16[16,64,512]{2,1,0:T(8,128)(2,1)S(1)} all-to-all(bf16[16,64,512]{2,1,0:T(8,128)(2,1)S(1)} %add_convert_fusion), channel_id=1, replica_groups=mesh['z'=8,'x'=4,'c'=2,'y'=4] {'x','y'}, dimensions={0} | all-to-all | bytes 2097152 | tf_op jit(solution)/shard_map/all_to_all | solution.py:27
  113.3 0.7 copy_bitcast_fusion
  114.0 3.4 %all-to-all-start.4 = ((bf16[8,16,512]{2,1,0:T(8,128)(2,1)}), bf16[8,16,512]{2,1,0:T(8,128)(2,1)S(1)}, u32[]{:S(2)}, u32[]{:S(2)}) async-start(bf16[8,16,512]{2,1,0:T(8,128)(2,1)} %copy_bitcast_fusion), calls=%async_computation.4 | async-start | bytes 262144 | tf_op jit(solution)/shard_map/all_to_all | solution.py:27
  118.0 7.3 %all-to-all-done.4 = bf16[8,16,512]{2,1,0:T(8,128)(2,1)S(1)} async-done(((bf16[8,16,512]{2,1,0:T(8,128)(2,1)}), bf16[8,16,512]{2,1,0:T(8,128)(2,1)S(1)}, u32[]{:S(2)}, u32[]{:S(2)}) %all-to-all-start.4) | async-done | bytes 131104 | tf_op jit(solution)/shard_map/all_to_all | solution.py:27
  125.3 0.8 fusion
  (29 shorter events, 3.1 us)
Async XLA Ops:
  22.1 10.2 %collective-permute-start.3 = (bf16[8,32,640]{2,1,0:T(8,128)(2,1)S(1)}, bf16[8,32,640]{2,1,0:T(8,128)(2,1)S(1)}, u32[]{:S(2)}, u32[]{:S(2)}) collective-permute-start(bf16[8,32,640]{2,1,0:T(8,128)(2,1)S(1)} %all_to_all.25.refs_4_), channel_id=1, source_target_pairs={{0,4},{4,0},{1,5},{5,1},{2,6},{6,2},{3,7},{7,3},{8,12},{12,8},{9,1... | collective-permute-start | bytes 983048 | tf_op jit(solution)/shard_map/ppermute | solution.py:23
  25.7 4.9 %collective-permute-start = (bf16[32,512]{1,0:T(8,128)(2,1)S(1)}, bf16[32,512]{1,0:T(8,128)(2,1)S(1)}, u32[]{:S(2)}, u32[]{:S(2)}) collective-permute-start(bf16[32,512]{1,0:T(8,128)(2,1)S(1)} %get-tuple-element.22), channel_id=1, source_target_pairs={{0,8},{8,16},{16,24},{24,0},{1,9},{9,17},{17,25},{25,1},{2,10},{10... | collective-permute-start | bytes 98312 | tf_op jit(solution)/shard_map/ppermute | solution.py:23
  27.0 4.6 %collective-permute-start.1 = (bf16[32,512]{1,0:T(8,128)(2,1)S(1)}, bf16[32,512]{1,0:T(8,128)(2,1)S(1)}, u32[]{:S(2)}, u32[]{:S(2)}) collective-permute-start(bf16[32,512]{1,0:T(8,128)(2,1)S(1)} %get-tuple-element.23), channel_id=1, source_target_pairs={{0,16},{8,24},{16,0},{24,8},{1,17},{9,25},{17,1},{25,9},{2,18},{10... | collective-permute-start | bytes 98312 | tf_op jit(solution)/shard_map/ppermute | solution.py:23
  29.4 2.9 %collective-permute-start.2 = (bf16[32,512]{1,0:T(8,128)(2,1)S(1)}, bf16[32,512]{1,0:T(8,128)(2,1)S(1)}, u32[]{:S(2)}, u32[]{:S(2)}) collective-permute-start(bf16[32,512]{1,0:T(8,128)(2,1)S(1)} %get-tuple-element.24), channel_id=1, source_target_pairs={{0,24},{8,0},{16,8},{24,16},{1,25},{9,1},{17,9},{25,17},{2,26},{10... | collective-permute-start | bytes 98312 | tf_op jit(solution)/shard_map/ppermute | solution.py:23
  32.6 4.4 %collective-permute-start.4 = (bf16[32,640]{1,0:T(8,128)(2,1)S(1)}, bf16[32,640]{1,0:T(8,128)(2,1)S(1)}, u32[]{:S(2)}, u32[]{:S(2)}) collective-permute-start(bf16[32,640]{1,0:T(8,128)(2,1)S(1)} %get-tuple-element.26), channel_id=1, source_target_pairs={{0,24},{8,0},{16,8},{24,16},{1,25},{9,1},{17,9},{25,17},{2,26},{10... | collective-permute-start | bytes 122888 | tf_op jit(solution)/shard_map/ppermute | solution.py:23
  34.9 4.5 %collective-permute-start.5 = (bf16[32,640]{1,0:T(8,128)(2,1)S(1)}, bf16[32,640]{1,0:T(8,128)(2,1)S(1)}, u32[]{:S(2)}, u32[]{:S(2)}) collective-permute-start(bf16[32,640]{1,0:T(8,128)(2,1)S(1)} %get-tuple-element.27), channel_id=1, source_target_pairs={{0,16},{8,24},{16,0},{24,8},{1,17},{9,25},{17,1},{25,9},{2,18},{10... | collective-permute-start | bytes 122888 | tf_op jit(solution)/shard_map/ppermute | solution.py:23
  34.9 4.5 %collective-permute-start.6 = (bf16[32,640]{1,0:T(8,128)(2,1)S(1)}, bf16[32,640]{1,0:T(8,128)(2,1)S(1)}, u32[]{:S(2)}, u32[]{:S(2)}) collective-permute-start(bf16[32,640]{1,0:T(8,128)(2,1)S(1)} %get-tuple-element.28), channel_id=1, source_target_pairs={{0,8},{8,16},{16,24},{24,0},{1,9},{9,17},{17,25},{25,1},{2,10},{10... | collective-permute-start | bytes 122888 | tf_op jit(solution)/shard_map/ppermute | solution.py:23
  39.4 15.5 %copy-start.3 = (bf16[32,2048]{1,0:T(8,128)(2,1)S(1)}, bf16[32,2048]{1,0:T(8,128)(2,1)}, u32[]{:S(2)}) copy-start(bf16[32,2048]{1,0:T(8,128)(2,1)} %refs_0_.3) | copy-start | bytes 393220
  39.4 15.5 %copy-start.4 = (f32[2048]{0:T(1024)S(1)}, f32[2048]{0:T(1024)}, u32[]{:S(2)}) copy-start(f32[2048]{0:T(1024)} %param.31) | copy-start | bytes 24580
  45.1 6.1 %collective-permute-start.9 = (bf16[32,2048]{1,0:T(8,128)(2,1)S(1)}, bf16[32,2048]{1,0:T(8,128)(2,1)S(1)}, u32[]{:S(2)}, u32[]{:S(2)}) collective-permute-start(bf16[32,2048]{1,0:T(8,128)(2,1)S(1)} %get-tuple-element.32), channel_id=1, source_target_pairs={{0,3},{1,0},{2,1},{3,2},{4,7},{5,4},{6,5},{7,6},{8,11},{9,8},{10,9... | collective-permute-start | bytes 393224 | tf_op jit(solution)/shard_map/ppermute | solution.py:23
  47.9 5.4 %collective-permute-start.8 = (bf16[32,2048]{1,0:T(8,128)(2,1)S(1)}, bf16[32,2048]{1,0:T(8,128)(2,1)S(1)}, u32[]{:S(2)}, u32[]{:S(2)}) collective-permute-start(bf16[32,2048]{1,0:T(8,128)(2,1)S(1)} %get-tuple-element.32), channel_id=1, source_target_pairs={{0,2},{1,3},{2,0},{3,1},{4,6},{5,7},{6,4},{7,5},{8,10},{9,11},{10,... | collective-permute-start | bytes 393224 | tf_op jit(solution)/shard_map/ppermute | solution.py:23
  48.3 6.4 %collective-permute-start.7 = (bf16[32,2048]{1,0:T(8,128)(2,1)S(1)}, bf16[32,2048]{1,0:T(8,128)(2,1)S(1)}, u32[]{:S(2)}, u32[]{:S(2)}) collective-permute-start(bf16[32,2048]{1,0:T(8,128)(2,1)S(1)} %get-tuple-element.32), channel_id=1, source_target_pairs={{0,1},{1,2},{2,3},{3,0},{4,5},{5,6},{6,7},{7,4},{8,9},{9,10},{10,1... | collective-permute-start | bytes 393224 | tf_op jit(solution)/shard_map/ppermute | solution.py:23
  55.1 34.9 %copy-start = (bf16[2048,256]{1,0:T(8,128)(2,1)S(1)}, bf16[2048,256]{1,0:T(8,128)(2,1)}, u32[]{:S(2)}) copy-start(bf16[2048,256]{1,0:T(8,128)(2,1)} %gate_ref.3) | copy-start | bytes 3145732
  55.1 34.9 %copy-start.1 = (bf16[2048,256]{1,0:T(8,128)(2,1)S(1)}, bf16[2048,256]{1,0:T(8,128)(2,1)}, u32[]{:S(2)}) copy-start(bf16[2048,256]{1,0:T(8,128)(2,1)} %up_ref.3) | copy-start | bytes 3145732
  55.1 34.9 %copy-start.2 = (bf16[256,2048]{1,0:T(8,128)(2,1)S(1)}, bf16[256,2048]{1,0:T(8,128)(2,1)}, u32[]{:S(2)}) copy-start(bf16[256,2048]{1,0:T(8,128)(2,1)} %down_ref.3) | copy-start | bytes 3145732
  80.6 9.4 %collective-permute-start.10 = (bf16[16,64,512]{2,1,0:T(8,128)(2,1)S(1)}, bf16[16,64,512]{2,1,0:T(8,128)(2,1)S(1)}, u32[]{:S(2)}, u32[]{:S(2)}) collective-permute-start(bf16[16,64,512]{2,1,0:T(8,128)(2,1)S(1)} %all_to_all.27.rows_ref), channel_id=1, source_target_pairs={{0,4},{4,0},{1,5},{5,1},{2,6},{6,2},{3,7},{7,3},{8,12},{12,8},{9,1... | collective-permute-start | bytes 3145736 | tf_op jit(solution)/shard_map/ppermute | solution.py:23
  91.1 2.8 %collective-permute-start.11 = (bf16[16,64,512]{2,1,0:T(8,128)(2,1)S(1)}, bf16[16,64,512]{2,1,0:T(8,128)(2,1)S(1)}, u32[]{:S(2)}, u32[]{:S(2)}) collective-permute-start(bf16[16,64,512]{2,1,0:T(8,128)(2,1)S(1)} %shard_map.215), channel_id=1, source_target_pairs={{0,4},{4,0},{1,5},{5,1},{2,6},{6,2},{3,7},{7,3},{8,12},{12,8},{9,1... | collective-permute-start | bytes 3145736 | tf_op jit(solution)/shard_map/ppermute | solution.py:23
  114.0 11.3 %all-to-all-start.4 = ((bf16[8,16,512]{2,1,0:T(8,128)(2,1)}), bf16[8,16,512]{2,1,0:T(8,128)(2,1)S(1)}, u32[]{:S(2)}, u32[]{:S(2)}) async-start(bf16[8,16,512]{2,1,0:T(8,128)(2,1)} %copy_bitcast_fusion), calls=%async_computation.4 | async-start | bytes 262144 | tf_op jit(solution)/shard_map/all_to_all | solution.py:27

commit v2 on v1

--- a/solution.py
+++ b/solution.py
@@ -27,41 +27,126 @@
     return lax.all_to_all(blocks, axis, split_axis=0, concat_axis=0, tiled=True)
 
 
-def inv_rms(field):
-    return lax.rsqrt(jnp.mean(field * field, axis=-1, keepdims=True) + EPSILON)
-
-
-def expert_kernel(nx, rows_ref, gate_ref, up_ref, down_ref, out_ref):
+def expert_kernel(nx, rows_ref, gate_refs, up_refs, down_refs, out_ref):
     blocks, part, width = rows_ref.shape
     ny = blocks // nx
-    gate = up = None
+    gates, ups = [None] * len(gate_refs), [None] * len(up_refs)
     for y in range(ny):
         taken = jnp.concatenate([rows_ref[x * ny + y] for x in range(nx)], axis=0)
         deep = pl.ds(y * width, width)
-        g = jnp.dot(taken, gate_ref[deep, :], preferred_element_type=F32)
-        u = jnp.dot(taken, up_ref[deep, :], preferred_element_type=F32)
-        gate, up = (g, u) if gate is None else (gate + g, up + u)
-    hidden = (gate / (1.0 + jnp.exp(-gate)) * up).astype(BF16)
+        for sums, refs in ((gates, gate_refs), (ups, up_refs)):
+            for k, ref in enumerate(refs):
+                one = jnp.dot(taken, ref[deep, :], preferred_element_type=F32)
+                sums[k] = one if sums[k] is None else sums[k] + one
+    hidden = [
+        (gate / (1.0 + jnp.exp(-gate)) * up).astype(BF16) for gate, up in zip(gates, ups)
+    ]
     for y in range(ny):
-        back = jnp.dot(hidden, down_ref[:, pl.ds(y * width, width)], preferred_element_type=F32)
+        wide = pl.ds(y * width, width)
+        back = None
+        for one, ref in zip(hidden, down_refs):
+            more = jnp.dot(one, ref[:, wide], preferred_element_type=F32)
+            back = more if back is None else back + more
         back = back.astype(BF16)
         for x in range(nx):
             out_ref[x * ny + y] = back[x * part : (x + 1) * part]
 
 
-def expert_rows(blocks, gate, up, down, nx):
+def expert_rows(blocks, gates, ups, downs, nx):
+    in_vmem = pl.BlockSpec(memory_space=pltpu.VMEM)
+    count = len(gates)
     return pl.pallas_call(
         functools.partial(expert_kernel, nx),
         out_shape=jax.ShapeDtypeStruct(blocks.shape, BF16),
-        in_specs=[pl.BlockSpec(memory_space=pltpu.VMEM)] * 4,
-        out_specs=pl.BlockSpec(memory_space=pltpu.VMEM),
-        compiler_params=pltpu.CompilerParams(vmem_limit_bytes=16 * 2**20),
+        in_specs=[in_vmem] + [[in_vmem] * count] * 3,
+        out_specs=in_vmem,
+        compiler_params=pltpu.CompilerParams(vmem_limit_bytes=20 * 2**20),
         cost_estimate=pl.CostEstimate(
-            flops=2 * blocks.size * 3 * gate.shape[1],
-            bytes_accessed=4 * blocks.size + 6 * gate.size,
+            flops=2 * blocks.size * 3 * count * gates[0].shape[1],
+            bytes_accessed=4 * blocks.size + 6 * count * gates[0].size,
             transcendentals=0,
         ),
-    )(blocks, gate, up, down)
+    )(blocks, gates, ups, downs)
+
+
+def settle_kernel(mix_refs, tokens_ref, gains_ref, selector_ref, packed_ref, cols_ref, whole_s):
+    mix = None
+    for ref in mix_refs:
+        one = ref[...].astype(F32)
+        mix = one if mix is None else mix + one
+    cols = cols_ref.shape[1]
+    mix = mix * lax.rsqrt(jnp.mean(mix * mix, axis=1, keepdims=True) + EPSILON)
+    whole = tokens_ref[...].astype(F32) + mix * gains_ref[pl.ds(0, 1), :]
+    whole_s[...] = whole
+    scale = lax.rsqrt(jnp.mean(whole * whole, axis=1, keepdims=True) + EPSILON)
+    here = pl.ds(pl.multiple_of(lax.axis_index("y") * cols, cols), cols)
+    residual = whole_s[:, here]
+    cols_ref[...] = residual
+    taken = (residual * scale * gains_ref[pl.ds(1, 1), here]).astype(BF16)
+    packed = jnp.dot(selector_ref[...], taken, preferred_element_type=F32)
+    packed_ref[...] = packed.astype(BF16)
+
+
+def settle(mixes, tokens, gains, selector, cols):
+    rows, width = tokens.shape
+    in_vmem = pl.BlockSpec(memory_space=pltpu.VMEM)
+    return pl.pallas_call(
+        settle_kernel,
+        out_shape=(
+            jax.ShapeDtypeStruct((selector.shape[0], cols), BF16),
+            jax.ShapeDtypeStruct((rows, cols), F32),
+        ),
+        in_specs=[[in_vmem] * len(mixes)] + [in_vmem] * 3,
+        out_specs=(in_vmem,) * 2,
+        scratch_shapes=[pltpu.VMEM((rows, width), F32)],
+        compiler_params=pltpu.CompilerParams(vmem_limit_bytes=6 * 2**20),
+    )(mixes, tokens, gains, selector)
+
+
+def fold_kernel(partials_ref, out_ref):
+    nz, slots, _ = out_ref.shape
+    blocks, rows, _ = partials_ref.shape
+    each = rows // nz
+    local_experts = slots // each
+    share = blocks // local_experts
+    for e in range(local_experts):
+        total = partials_ref[e * share].astype(F32)
+        for k in range(1, share):
+            total = total + partials_ref[e * share + k].astype(F32)
+        total = total.astype(BF16)
+        for z in range(nz):
+            out_ref[z, pl.ds(e * each, each), :] = total[z * each : (z + 1) * each]
+
+
+def fold_partials(partials, local_experts, nz):
+    _, rows, cols = partials.shape
+    return pl.pallas_call(
+        fold_kernel,
+        out_shape=jax.ShapeDtypeStruct((nz, local_experts * rows // nz, cols), BF16),
+        in_specs=[pl.BlockSpec(memory_space=pltpu.VMEM)],
+        out_specs=pl.BlockSpec(memory_space=pltpu.VMEM),
+        compiler_params=pltpu.CompilerParams(vmem_limit_bytes=6 * 2**20),
+    )(partials)
+
+
+def join_kernel(query_ref, key_ref, value_ref, out_ref, query_s, key_s, value_s, sems):
+    parts = fetched((query_ref, key_ref, value_ref), (query_s, key_s, value_s), sems)
+    joined = jnp.concatenate([part[...] for part in parts], axis=1)
+    for k in range(out_ref.shape[0]):
+        out_ref[k] = joined
+
+
+def join(arrays, copies):
+    rows = arrays[0].shape[0]
+    cols = sum(array.shape[1] for array in arrays)
+    return pl.pallas_call(
+        join_kernel,
+        out_shape=jax.ShapeDtypeStruct((copies, rows, cols), BF16),
+        in_specs=[pl.BlockSpec(memory_space=pltpu.HBM)] * 3,
+        out_specs=pl.BlockSpec(memory_space=pltpu.VMEM),
+        scratch_shapes=places_for(arrays),
+        compiler_params=pltpu.CompilerParams(vmem_limit_bytes=4 * 2**20),
+    )(*in_hbm(*arrays))
 
 
 def attend_kernel(
@@ -319,16 +404,30 @@
 
 
 def early_kernel(count, *refs):
-    scale_ref, log_gate_ref, gate_ref, long_ref, selector_ref, weighing_ref = refs[count : count + 6]
+    (
+        scale_ref,
+        log_gate_ref,
+        gate_ref,
+        long_ref,
+        selector_ref,
+        weighing_ref,
+        kept_ref,
+        gains_ref,
+    ) = refs[count : count + 8]
     (
         tokens_ref,
         gain_ref,
+        gain_mix_ref,
+        gain_ffn_ref,
         forget_ref,
         bias_ref,
         length_ref,
         routes_ref,
         weights_ref,
-    ) = fetched(refs[:count], refs[count + 6 : -1], refs[-1])
+    ) = fetched(refs[:count], refs[count + 8 : -1], refs[-1])
+    kept_ref[...] = tokens_ref[...]
+    gains_ref[pl.ds(0, 1), :] = gain_mix_ref[...]
+    gains_ref[pl.ds(1, 1), :] = gain_ffn_ref[...]
 
     tokens = tokens_ref[...].astype(F32)
     rows = tokens.shape[0]
@@ -378,7 +477,7 @@
 
 def early(*arrays):
     in_vmem = pl.BlockSpec(memory_space=pltpu.VMEM)
-    tokens, _, forget, *_ = arrays
+    tokens, _, _, _, forget, *_ = arrays
     rows, group = tokens.shape[0], forget.shape[0]
     slots = EXPERTS * CAP
     return pl.pallas_call(
@@ -390,9 +489,11 @@
             jax.ShapeDtypeStruct((rows, group, 1), jnp.int32),
             jax.ShapeDtypeStruct((slots, rows), BF16),
             jax.ShapeDtypeStruct((slots, rows), F32),
+            jax.ShapeDtypeStruct(tokens.shape, BF16),
+            jax.ShapeDtypeStruct((2, tokens.shape[1]), F32),
         ),
         in_specs=[pl.BlockSpec(memory_space=pltpu.HBM)] * len(arrays),
-        out_specs=(in_vmem,) * 6,
+        out_specs=(in_vmem,) * 8,
         scratch_shapes=places_for(arrays),
         compiler_params=pltpu.CompilerParams(vmem_limit_bytes=6 * 2**20),
     )(*in_hbm(*arrays))
@@ -421,11 +522,12 @@
 ):
     _, width = tokens.shape
     nz, nx, _, ny = (lax.axis_size(a) for a in ("z", "x", "c", "y"))
-    iy = lax.axis_index("y")
-
-    scale_attn, new_log_gate, gate, long, selector, weighing = early(
+
+    scale_attn, new_log_gate, gate, long, selector, weighing, kept, gains = early(
         tokens,
         norm_gain_attn.reshape(1, width),
+        norm_gain_mix.reshape(1, width),
+        norm_gain_ffn.reshape(1, width),
         w_forget.T,
         forget_bias.reshape(1, -1),
         lengths.reshape(1, -1),
@@ -433,8 +535,9 @@
         route_weights.T,
     )
 
-    weights = jnp.concatenate((w_query, w_key, w_value), axis=1)
-    same_core = exchange(jnp.broadcast_to(weights, (nz, *weights.shape)), "z")
+    weights = join((w_query, w_key, w_value), nz)
+    same_core = exchange(weights, "z")
+    others = [shifted(w, "c", 1) for w in (expert_gate, expert_up, expert_down)]
     other_core = shifted(same_core, "c", 1)
     mine = cut_tokens(tokens, norm_gain_attn.reshape(1, width), nz, nx)
     moved = [shifted(mine[s], "x", s) for s in range(1, nx)]
@@ -453,19 +556,10 @@
         w_out,
     )
 
-    residual = tokens.astype(F32)
-    others = [shifted(partial_mix, "y", s) for s in range(1, ny)]
-    mix = partial_mix.astype(F32)
-    for other in others:
-        mix = mix + other.astype(F32)
-    mixed_res = residual + mix * inv_rms(mix) * norm_gain_mix
+    mixes = [partial_mix] + [shifted(partial_mix, "y", s) for s in range(1, ny)]
     col_width = width // ny
-    scale_ffn = inv_rms(mixed_res)
-    residual_cols = lax.dynamic_slice_in_dim(mixed_res, iy * col_width, col_width, 1)
-    gain_ffn_cols = lax.dynamic_slice_in_dim(norm_gain_ffn, iy * col_width, col_width, 0)
-    ffn_cols = (residual_cols * scale_ffn * gain_ffn_cols).astype(BF16)
-
-    packed = jnp.dot(selector, ffn_cols, preferred_element_type=F32).astype(BF16)
+    packed, residual_cols = settle(mixes, kept, gains, selector, col_width)
+
     local_experts = EXPERTS // nz
     spread = nx // local_experts
     on_z = exchange(packed.reshape(nz, local_experts * CAP, col_width), "z")
@@ -473,14 +567,9 @@
     on_z = on_z.reshape(local_experts, 1, 1, nz * CAP, col_width)
     outgoing = jnp.broadcast_to(on_z, (local_experts, spread, ny, nz * CAP, col_width))
     own = exchange(outgoing.reshape(nx * ny, nz * CAP, col_width), ("x", "y"))
-    other = shifted(own, "c", 1)
-    own_part = expert_rows(own, expert_gate, expert_up, expert_down, nx)
-    other_part = expert_rows(other, expert_gate, expert_up, expert_down, nx)
-    both = own_part.astype(F32) + shifted(other_part, "c", 1).astype(F32)
-    summed = exchange(both.astype(BF16), ("x", "y"))
-    summed = summed.reshape(local_experts, spread * ny, nz, CAP, col_width).astype(F32)
-    summed = jnp.sum(summed, axis=1).astype(BF16).transpose(1, 0, 2, 3)
-    returned = exchange(summed.reshape(nz, local_experts * CAP, col_width), "z")
+    part = expert_rows(own, *[list(p) for p in zip((expert_gate, expert_up, expert_down), others)], nx)
+    summed = exchange(part, ("x", "y"))
+    returned = exchange(fold_partials(summed, local_experts, nz), "z")
     returned = returned.reshape(EXPERTS * CAP, col_width)
     routed = lax.dot_general(
         weighing, returned.astype(F32), (((0,), (0,)), ((), ())), preferred_element_type=F32

time: 127 us -> 126 us (level)
  the two profiles are of different devices: /device:TPU:1 before, /device:TPU:8 now
where the time goes in v2:
time: 126 us; the launch traced here: 125 us
  blocking collectives  37.8 us (30%)
  waiting for transfers between devices  37.6 us (30%)
  starting transfers between devices  31.4 us (25%)
  Pallas kernels  15.3 us (12%)
  local copies, waits for them, and re-layouts  1.74 us (1%)
    all_to_all x2, blocking collectives, exchange(): return lax.all_to_all(blocks, axis, split_axis=0, concat_axis=0, tiled=True)  37.8 us
    all_to_all x3, waiting for transfers between devices, exchange(): return lax.all_to_all(blocks, axis, split_axis=0, concat_axis=0, tiled=True)  28.3 us
    all_to_all x3, starting transfers between devices, exchange(): return lax.all_to_all(blocks, axis, split_axis=0, concat_axis=0, tiled=True)  16.3 us
    ppermute x13, starting transfers between devices, shifted(): return lax.ppermute(value, axis, [(i, (i + step) % n) for i in range(n)])  15.1 us
    ppermute x13, waiting for transfers between devices, shifted(): return lax.ppermute(value, axis, [(i, (i + step) % n) for i in range(n)])  9.29 us
    pallas_call x1, Pallas kernels, attend(): pl.pallas_call(functools.partial(attend_kernel, together, parts), out_sha...  5.82 us
    pallas_call x1, Pallas kernels, expert_rows(): pl.pallas_call(functools.partial(expert_kernel, nx), out_shape=jax.ShapeD...  4.04 us
  transfers between devices with their start and end apart: 16, of which 9 were waited for; matrix products, arithmetic and copies ran while one was open for 1% of the time, Pallas kernels for 2%

profile of v2, /device:TPU:8, one launch (start us, length us, event | category | flops | bytes accessed | tf_op | source)
XLA Modules:
  0.0 125.4 jit_solution(10604787240268918009)
XLA Ops:
  0.6 0.9 shard_map.211
  1.5 21.5 %all_to_all.25.refs_4_ = bf16[8,32,640]{2,1,0:T(8,128)(2,1)S(1)} all-to-all(bf16[8,32,640]{2,1,0:T(8,128)(2,1)S(1)} %shard_map.211), channel_id=1, replica_groups=mesh['z'=8,'x'=4,'c'=2,'y'=4] {'z'}, dimensions={0} | all-to-all | bytes 655360 | tf_op jit(solution)/shard_map/all_to_all | solution.py:27
  23.1 1.1 shard_map.210
  24.1 1.6 %collective-permute-start = (bf16[32,512]{1,0:T(8,128)(2,1)S(1)}, bf16[32,512]{1,0:T(8,128)(2,1)S(1)}, u32[]{:S(2)}, u32[]{:S(2)}) collective-permute-start(bf16[32,512]{1,0:T(8,128)(2,1)S(1)} %get-tuple-element.26), channel_id=1, source_target_pairs={{0,8},{8,16},{16,24},{24,0},{1,9},{9,17},{17,25},{25,1},{2,10},{10... | collective-permute-start | bytes 98312 | tf_op jit(solution)/shard_map/ppermute | solution.py:23
  25.7 2.7 %collective-permute-start.1 = (bf16[32,512]{1,0:T(8,128)(2,1)S(1)}, bf16[32,512]{1,0:T(8,128)(2,1)S(1)}, u32[]{:S(2)}, u32[]{:S(2)}) collective-permute-start(bf16[32,512]{1,0:T(8,128)(2,1)S(1)} %get-tuple-element.27), channel_id=1, source_target_pairs={{0,16},{8,24},{16,0},{24,8},{1,17},{9,25},{17,1},{25,9},{2,18},{10... | collective-permute-start | bytes 98312 | tf_op jit(solution)/shard_map/ppermute | solution.py:23
  28.4 1.4 %collective-permute-start.2 = (bf16[32,512]{1,0:T(8,128)(2,1)S(1)}, bf16[32,512]{1,0:T(8,128)(2,1)S(1)}, u32[]{:S(2)}, u32[]{:S(2)}) collective-permute-start(bf16[32,512]{1,0:T(8,128)(2,1)S(1)} %get-tuple-element.28), channel_id=1, source_target_pairs={{0,24},{8,0},{16,8},{24,16},{1,25},{9,1},{17,9},{25,17},{2,26},{10... | collective-permute-start | bytes 98312 | tf_op jit(solution)/shard_map/ppermute | solution.py:23
  29.9 1.3 collective-permute-done.1.refs_2_
  31.1 1.2 collective-permute-done.2.refs_3_
  32.7 2.7 %collective-permute-start.4 = (bf16[32,640]{1,0:T(8,128)(2,1)S(1)}, bf16[32,640]{1,0:T(8,128)(2,1)S(1)}, u32[]{:S(2)}, u32[]{:S(2)}) collective-permute-start(bf16[32,640]{1,0:T(8,128)(2,1)S(1)} %get-tuple-element.30), channel_id=1, source_target_pairs={{0,24},{8,0},{16,8},{24,16},{1,25},{9,1},{17,9},{25,17},{2,26},{10... | collective-permute-start | bytes 122888 | tf_op jit(solution)/shard_map/ppermute | solution.py:23
  35.4 1.0 collective-permute-start.6
  36.3 1.4 %shard_map.213 = (f32[32,1]{1,0:T(8,128)S(1)}, f32[32,8]{1,0:T(8,128)S(1)}, f32[32,8,1]{2,1,0:T(8,128)S(1)}, s32[32,8,1]{2,1,0:T(8,128)S(1)}, bf16[128,32]{1,0:T...) custom-call(bf16[32,2048]{1,0:T(8,128)(2,1)} %refs_0_.3, ...), custom_call_target="tpu_custom_call" | custom-call | tf_op jit(solution)/shard_map/pallas_call | solution.py:483
  37.8 3.2 %collective-permute-done.5.pieces_refs_1_ = bf16[32,640]{1,0:T(8,128)(2,1)S(1)} collective-permute-done((bf16[32,640]{1,0:T(8,128)(2,1)S(1)}, bf16[32,640]{1,0:T(8,128)(2,1)S(1)}, u32[]{:S(2)}, u32[]{:S(2)}) %collective-permute-start.5) | collective-permute-done | bytes 40992 | tf_op jit(solution)/shard_map/ppermute | solution.py:23
  41.0 5.8 %shard_map.214 = (bf16[32,2048]{1,0:T(8,128)(2,1)S(1)}, bf16[32,64]{1,0:T(8,128)(2,1)}, bf16[32,64]{1,0:T(8,128)(2,1)}) custom-call(f32[32,640]{1,0:T(8,128)S(1)} %get-tuple-element.29.own_ref, bf16[32,640]{1,0:T(8,128)(2,1)S(1)} %collective-permute-done.4.pieces_refs_0_, bf16[32,640]{1,0:T(8,128)(2,1)S(1)} %collective-permute-done.5.pieces_refs_1_, ...), custom_call_target="tpu_custom_call" | custom-call | flops 134217728 | bytes 11534336 | tf_op jit(solution)/shard_map/pallas_call | solution.py:296
  46.9 0.5 collective-permute-start.9
  47.4 2.6 %collective-permute-start.8 = (bf16[32,2048]{1,0:T(8,128)(2,1)S(1)}, bf16[32,2048]{1,0:T(8,128)(2,1)S(1)}, u32[]{:S(2)}, u32[]{:S(2)}) collective-permute-start(bf16[32,2048]{1,0:T(8,128)(2,1)S(1)} %get-tuple-element.36.mix_refs_0_), channel_id=1, source_target_pairs={{0,2},{1,3},{2,0},{3,1},{4,6},{5,7},{6,4},{7,5},{8,10},{9,11},{10,... | collective-permute-start | bytes 393224 | tf_op jit(solution)/shard_map/ppermute | solution.py:23
  50.0 1.9 %collective-permute-start.7 = (bf16[32,2048]{1,0:T(8,128)(2,1)S(1)}, bf16[32,2048]{1,0:T(8,128)(2,1)S(1)}, u32[]{:S(2)}, u32[]{:S(2)}) collective-permute-start(bf16[32,2048]{1,0:T(8,128)(2,1)S(1)} %get-tuple-element.36.mix_refs_0_), channel_id=1, source_target_pairs={{0,1},{1,2},{2,3},{3,0},{4,5},{5,6},{6,7},{7,4},{8,9},{9,10},{10,1... | collective-permute-start | bytes 393224 | tf_op jit(solution)/shard_map/ppermute | solution.py:23
  52.1 2.2 %collective-permute-done.8.mix_refs_2_ = bf16[32,2048]{1,0:T(8,128)(2,1)S(1)} collective-permute-done((bf16[32,2048]{1,0:T(8,128)(2,1)S(1)}, bf16[32,2048]{1,0:T(8,128)(2,1)S(1)}, u32[]{:S(2)}, u32[]{:S(2)}) %collective-permute-start.8) | collective-permute-done | bytes 131104 | tf_op jit(solution)/shard_map/ppermute | solution.py:23
  54.3 1.1 collective-permute-done.7.mix_refs_1_
  55.4 1.1 shard_map.215
  56.5 3.4 %all-to-all-start.1 = ((bf16[8,16,512]{2,1,0:T(8,128)(2,1)}), bf16[8,16,512]{2,1,0:T(8,128)(2,1)S(1)}, u32[]{:S(2)}, u32[]{:S(2)}) async-start(bf16[8,16,512]{2,1,0:T(8,128)(2,1)} %bitcast.8), calls=%async_computation.1 | async-start | bytes 262144 | tf_op jit(solution)/shard_map/all_to_all | solution.py:27
  60.0 0.5 collective-permute-start.11
  60.6 8.3 %all-to-all-done.1 = bf16[8,16,512]{2,1,0:T(8,128)(2,1)S(1)} async-done(((bf16[8,16,512]{2,1,0:T(8,128)(2,1)}), bf16[8,16,512]{2,1,0:T(8,128)(2,1)S(1)}, u32[]{:S(2)}, u32[]{:S(2)}) %all-to-all-start.1) | async-done | bytes 131104 | tf_op jit(solution)/shard_map/all_to_all | solution.py:27
  68.8 1.1 broadcast_in_dim.8
  69.9 6.3 %all-to-all-start.2 = ((bf16[16,64,512]{2,1,0:T(8,128)(2,1)}), bf16[16,64,512]{2,1,0:T(8,128)(2,1)S(1)}, u32[]{:S(2)}, u32[]{:S(2)}) async-start(bf16[16,64,512]{2,1,0:T(8,128)(2,1)} %bitcast.20), calls=%async_computation.2 | async-start | bytes 2097152 | tf_op jit(solution)/shard_map/all_to_all | solution.py:27
  76.3 11.6 %all-to-all-done.2.rows_ref = bf16[16,64,512]{2,1,0:T(8,128)(2,1)S(1)} async-done(((bf16[16,64,512]{2,1,0:T(8,128)(2,1)}), bf16[16,64,512]{2,1,0:T(8,128)(2,1)S(1)}, u32[]{:S(2)}, u32[]{:S(2)}) %all-to-all-start.2) | async-done | bytes 1048608 | tf_op jit(solution)/shard_map/all_to_all | solution.py:27
  87.9 4.0 %shard_map.216 = bf16[16,64,512]{2,1,0:T(8,128)(2,1)S(1)} custom-call(bf16[16,64,512]{2,1,0:T(8,128)(2,1)S(1)} %all-to-all-done.2.rows_ref, bf16[2048,256]{1,0:T(8,128)(2,1)S(1)} %copy-done, bf16[2048,256]{1,0:T(8,128)(2,1)} %collective-permute-done.10.gate_refs_1_, bf16[2048,256]{1,0:T(8,128)(2,1)S(1)} %copy-done.1, ...), custom_call_target="tpu_custom_call" | custom-call | flops 1610612736 | bytes 8388608 | tf_op jit(solution)/shard_map/pallas_call | solution.py:58
  91.9 16.2 %all_to_all.26.partials_ref = bf16[16,64,512]{2,1,0:T(8,128)(2,1)S(1)} all-to-all(bf16[16,64,512]{2,1,0:T(8,128)(2,1)S(1)} %shard_map.216), channel_id=1, replica_groups=mesh['z'=8,'x'=4,'c'=2,'y'=4] {'x','y'}, dimensions={0} | all-to-all | bytes 2097152 | tf_op jit(solution)/shard_map/all_to_all | solution.py:27
  108.2 0.8 shard_map.217
  109.0 6.5 %all-to-all-start.4 = ((bf16[8,16,512]{2,1,0:T(8,128)(2,1)}), bf16[8,16,512]{2,1,0:T(8,128)(2,1)S(1)}, u32[]{:S(2)}, u32[]{:S(2)}) async-start(bf16[8,16,512]{2,1,0:T(8,128)(2,1)} %shard_map.217), calls=%async_computation.4 | async-start | bytes 262144 | tf_op jit(solution)/shard_map/all_to_all | solution.py:27
  115.5 0.7 copy.24
  116.2 8.4 %all-to-all-done.4 = bf16[8,16,512]{2,1,0:T(8,128)(2,1)S(1)} async-done(((bf16[8,16,512]{2,1,0:T(8,128)(2,1)}), bf16[8,16,512]{2,1,0:T(8,128)(2,1)S(1)}, u32[]{:S(2)}, u32[]{:S(2)}) %all-to-all-start.4) | async-done | bytes 131104 | tf_op jit(solution)/shard_map/all_to_all | solution.py:27
  124.8 0.6 add_convert_fusion
  (19 shorter events, 1.0 us)
Async XLA Ops:
  23.1 9.3 %collective-permute-start.3 = (bf16[8,32,640]{2,1,0:T(8,128)(2,1)S(1)}, bf16[8,32,640]{2,1,0:T(8,128)(2,1)S(1)}, u32[]{:S(2)}, u32[]{:S(2)}) collective-permute-start(bf16[8,32,640]{2,1,0:T(8,128)(2,1)S(1)} %all_to_all.25.refs_4_), channel_id=1, source_target_pairs={{0,4},{4,0},{1,5},{5,1},{2,6},{6,2},{3,7},{7,3},{8,12},{12,8},{9,1... | collective-permute-start | bytes 983048 | tf_op jit(solution)/shard_map/ppermute | solution.py:23
  24.1 5.7 %collective-permute-start = (bf16[32,512]{1,0:T(8,128)(2,1)S(1)}, bf16[32,512]{1,0:T(8,128)(2,1)S(1)}, u32[]{:S(2)}, u32[]{:S(2)}) collective-permute-start(bf16[32,512]{1,0:T(8,128)(2,1)S(1)} %get-tuple-element.26), channel_id=1, source_target_pairs={{0,8},{8,16},{16,24},{24,0},{1,9},{9,17},{17,25},{25,1},{2,10},{10... | collective-permute-start | bytes 98312 | tf_op jit(solution)/shard_map/ppermute | solution.py:23
  25.7 5.4 %collective-permute-start.1 = (bf16[32,512]{1,0:T(8,128)(2,1)S(1)}, bf16[32,512]{1,0:T(8,128)(2,1)S(1)}, u32[]{:S(2)}, u32[]{:S(2)}) collective-permute-start(bf16[32,512]{1,0:T(8,128)(2,1)S(1)} %get-tuple-element.27), channel_id=1, source_target_pairs={{0,16},{8,24},{16,0},{24,8},{1,17},{9,25},{17,1},{25,9},{2,18},{10... | collective-permute-start | bytes 98312 | tf_op jit(solution)/shard_map/ppermute | solution.py:23
  28.4 3.9 %collective-permute-start.2 = (bf16[32,512]{1,0:T(8,128)(2,1)S(1)}, bf16[32,512]{1,0:T(8,128)(2,1)S(1)}, u32[]{:S(2)}, u32[]{:S(2)}) collective-permute-start(bf16[32,512]{1,0:T(8,128)(2,1)S(1)} %get-tuple-element.28), channel_id=1, source_target_pairs={{0,24},{8,0},{16,8},{24,16},{1,25},{9,1},{17,9},{25,17},{2,26},{10... | collective-permute-start | bytes 98312 | tf_op jit(solution)/shard_map/ppermute | solution.py:23
  32.7 5.1 %collective-permute-start.4 = (bf16[32,640]{1,0:T(8,128)(2,1)S(1)}, bf16[32,640]{1,0:T(8,128)(2,1)S(1)}, u32[]{:S(2)}, u32[]{:S(2)}) collective-permute-start(bf16[32,640]{1,0:T(8,128)(2,1)S(1)} %get-tuple-element.30), channel_id=1, source_target_pairs={{0,24},{8,0},{16,8},{24,16},{1,25},{9,1},{17,9},{25,17},{2,26},{10... | collective-permute-start | bytes 122888 | tf_op jit(solution)/shard_map/ppermute | solution.py:23
  35.4 5.6 %collective-permute-start.5 = (bf16[32,640]{1,0:T(8,128)(2,1)S(1)}, bf16[32,640]{1,0:T(8,128)(2,1)S(1)}, u32[]{:S(2)}, u32[]{:S(2)}) collective-permute-start(bf16[32,640]{1,0:T(8,128)(2,1)S(1)} %get-tuple-element.31), channel_id=1, source_target_pairs={{0,16},{8,24},{16,0},{24,8},{1,17},{9,25},{17,1},{25,9},{2,18},{10... | collective-permute-start | bytes 122888 | tf_op jit(solution)/shard_map/ppermute | solution.py:23
  35.4 5.7 %collective-permute-start.6 = (bf16[32,640]{1,0:T(8,128)(2,1)S(1)}, bf16[32,640]{1,0:T(8,128)(2,1)S(1)}, u32[]{:S(2)}, u32[]{:S(2)}) collective-permute-start(bf16[32,640]{1,0:T(8,128)(2,1)S(1)} %get-tuple-element.32), channel_id=1, source_target_pairs={{0,8},{8,16},{16,24},{24,0},{1,9},{9,17},{17,25},{25,1},{2,10},{10... | collective-permute-start | bytes 122888 | tf_op jit(solution)/shard_map/ppermute | solution.py:23
  41.0 18.8 %copy-start = (bf16[2048,256]{1,0:T(8,128)(2,1)S(1)}, bf16[2048,256]{1,0:T(8,128)(2,1)}, u32[]{:S(2)}) copy-start(bf16[2048,256]{1,0:T(8,128)(2,1)} %gate_refs_0_.1) | copy-start | bytes 3145732
  41.0 18.9 %copy-start.1 = (bf16[2048,256]{1,0:T(8,128)(2,1)S(1)}, bf16[2048,256]{1,0:T(8,128)(2,1)}, u32[]{:S(2)}) copy-start(bf16[2048,256]{1,0:T(8,128)(2,1)} %up_refs_0_.1) | copy-start | bytes 3145732
  46.9 5.3 %collective-permute-start.9 = (bf16[32,2048]{1,0:T(8,128)(2,1)S(1)}, bf16[32,2048]{1,0:T(8,128)(2,1)S(1)}, u32[]{:S(2)}, u32[]{:S(2)}) collective-permute-start(bf16[32,2048]{1,0:T(8,128)(2,1)S(1)} %get-tuple-element.36.mix_refs_0_), channel_id=1, source_target_pairs={{0,3},{1,0},{2,1},{3,2},{4,7},{5,4},{6,5},{7,6},{8,11},{9,8},{10,9... | collective-permute-start | bytes 393224 | tf_op jit(solution)/shard_map/ppermute | solution.py:23
  47.4 6.9 %collective-permute-start.8 = (bf16[32,2048]{1,0:T(8,128)(2,1)S(1)}, bf16[32,2048]{1,0:T(8,128)(2,1)S(1)}, u32[]{:S(2)}, u32[]{:S(2)}) collective-permute-start(bf16[32,2048]{1,0:T(8,128)(2,1)S(1)} %get-tuple-element.36.mix_refs_0_), channel_id=1, source_target_pairs={{0,2},{1,3},{2,0},{3,1},{4,6},{5,7},{6,4},{7,5},{8,10},{9,11},{10,... | collective-permute-start | bytes 393224 | tf_op jit(solution)/shard_map/ppermute | solution.py:23
  50.0 5.4 %collective-permute-start.7 = (bf16[32,2048]{1,0:T(8,128)(2,1)S(1)}, bf16[32,2048]{1,0:T(8,128)(2,1)S(1)}, u32[]{:S(2)}, u32[]{:S(2)}) collective-permute-start(bf16[32,2048]{1,0:T(8,128)(2,1)S(1)} %get-tuple-element.36.mix_refs_0_), channel_id=1, source_target_pairs={{0,1},{1,2},{2,3},{3,0},{4,5},{5,6},{6,7},{7,4},{8,9},{9,10},{10,1... | collective-permute-start | bytes 393224 | tf_op jit(solution)/shard_map/ppermute | solution.py:23
  56.5 12.4 %all-to-all-start.1 = ((bf16[8,16,512]{2,1,0:T(8,128)(2,1)}), bf16[8,16,512]{2,1,0:T(8,128)(2,1)S(1)}, u32[]{:S(2)}, u32[]{:S(2)}) async-start(bf16[8,16,512]{2,1,0:T(8,128)(2,1)} %bitcast.8), calls=%async_computation.1 | async-start | bytes 262144 | tf_op jit(solution)/shard_map/all_to_all | solution.py:27
  59.8 16.4 %collective-permute-start.10 = (bf16[2048,256]{1,0:T(8,128)(2,1)S(1)}, bf16[2048,256]{1,0:T(8,128)(2,1)}, u32[]{:S(2)}, u32[]{:S(2)}) collective-permute-start(bf16[2048,256]{1,0:T(8,128)(2,1)S(1)} %copy-done), channel_id=1, source_target_pairs={{0,4},{4,0},{1,5},{5,1},{2,6},{6,2},{3,7},{7,3},{8,12},{12,8},{9,1... | collective-permute-start | bytes 3145736 | tf_op jit(solution)/shard_map/ppermute | solution.py:23
  60.0 16.3 %collective-permute-start.11 = (bf16[2048,256]{1,0:T(8,128)(2,1)S(1)}, bf16[2048,256]{1,0:T(8,128)(2,1)}, u32[]{:S(2)}, u32[]{:S(2)}) collective-permute-start(bf16[2048,256]{1,0:T(8,128)(2,1)S(1)} %copy-done.1), channel_id=1, source_target_pairs={{0,4},{4,0},{1,5},{5,1},{2,6},{6,2},{3,7},{7,3},{8,12},{12,8},{9,1... | collective-permute-start | bytes 3145736 | tf_op jit(solution)/shard_map/ppermute | solution.py:23
  60.4 15.8 %collective-permute-start.12 = (bf16[256,2048]{1,0:T(8,128)(2,1)}, bf16[256,2048]{1,0:T(8,128)(2,1)}, u32[]{:S(2)}, u32[]{:S(2)}) collective-permute-start(bf16[256,2048]{1,0:T(8,128)(2,1)} %down_refs_0_.1), channel_id=1, source_target_pairs={{0,4},{4,0},{1,5},{5,1},{2,6},{6,2},{3,7},{7,3},{8,12},{12,8},{9,1... | collective-permute-start | bytes 3145736 | tf_op jit(solution)/shard_map/ppermute | solution.py:23
  69.9 18.0 %all-to-all-start.2 = ((bf16[16,64,512]{2,1,0:T(8,128)(2,1)}), bf16[16,64,512]{2,1,0:T(8,128)(2,1)S(1)}, u32[]{:S(2)}, u32[]{:S(2)}) async-start(bf16[16,64,512]{2,1,0:T(8,128)(2,1)} %bitcast.20), calls=%async_computation.2 | async-start | bytes 2097152 | tf_op jit(solution)/shard_map/all_to_all | solution.py:27
  109.0 15.6 %all-to-all-start.4 = ((bf16[8,16,512]{2,1,0:T(8,128)(2,1)}), bf16[8,16,512]{2,1,0:T(8,128)(2,1)S(1)}, u32[]{:S(2)}, u32[]{:S(2)}) async-start(bf16[8,16,512]{2,1,0:T(8,128)(2,1)} %shard_map.217), calls=%async_computation.4 | async-start | bytes 262144 | tf_op jit(solution)/shard_map/all_to_all | solution.py:27

commit v3 on v2

--- a/solution.py
+++ b/solution.py
@@ -169,10 +169,8 @@
     weight_s,
     heads_s,
     past_s,
-    cum_s,
     keys_s,
     values_s,
-    out_w_s,
     sems,
 ):
     rows, group, head_dim = q_s.shape
@@ -189,15 +187,9 @@
         ]
 
     key_copies = copies(0, keys_ref, keys_s)
-    cum_copies = copies(1, cum_ref, cum_s)
-    value_copies = copies(2, values_ref, values_s)
-    out_w_copy = pltpu.make_async_copy(out_w_ref, out_w_s, sems.at[3, 0])
-    for p in range(parts):
-        cum_copies[p].start()
-        key_copies[p].start()
-    for copy in value_copies:
+    value_copies = copies(1, values_ref, values_s)
+    for copy in key_copies + value_copies:
         copy.start()
-    out_w_copy.start()
 
     projected = own_ref[...]
     for ref in pieces_refs:
@@ -234,7 +226,7 @@
             for b in some
         ]
         lengths = [length_ref[b] for b in some]
-        cums = [cum_s[b] for b in some]
+        cums = [cum_ref[b] for b in some]
         lasts = [
             jnp.sum(jnp.where(places == n - 1, cum, 0.0), axis=1, keepdims=True)
             for n, cum in zip(lengths, cums)
@@ -269,7 +261,6 @@
             heads_s[b] = one
 
     for p in range(parts):
-        cum_copies[p].wait()
         key_copies[p].wait()
         for first in range(p * share, (p + 1) * share, together):
             weigh(range(first, first + together))
@@ -282,8 +273,22 @@
     wide = lax.dot_general(heads, fold, (((1,), (1,)), ((), ())), preferred_element_type=F32)
     wide = jnp.where(on_head, wide.reshape(rows, group, cols), 0.0)
     heads_out = jnp.sum(wide, axis=1).astype(BF16)
-    out_w_copy.wait()
-    mix_ref[...] = jnp.dot(heads_out, out_w_s[...], preferred_element_type=F32).astype(BF16)
+    mix_ref[...] = jnp.dot(heads_out, out_w_ref[...], preferred_element_type=F32).astype(BF16)
+
+
+def load_kernel(count, *refs):
+    fetched(refs[:count], refs[count:-1], refs[-1])
+
+
+def load(*arrays):
+    return pl.pallas_call(
+        functools.partial(load_kernel, len(arrays)),
+        out_shape=[jax.ShapeDtypeStruct(array.shape, array.dtype) for array in arrays],
+        in_specs=[pl.BlockSpec(memory_space=pltpu.HBM)] * len(arrays),
+        out_specs=[pl.BlockSpec(memory_space=pltpu.VMEM)] * len(arrays),
+        scratch_shapes=[pltpu.SemaphoreType.DMA((len(arrays),))],
+        compiler_params=pltpu.CompilerParams(vmem_limit_bytes=8 * 2**20),
+    )(*in_hbm(*arrays))
 
 
 def attend(own, pieces, scale, gate, lengths, cum, keys, values, out_w):
@@ -296,7 +301,10 @@
     return pl.pallas_call(
         functools.partial(attend_kernel, together, parts),
         out_shape=(jax.ShapeDtypeStruct((rows, width), BF16), one, one),
-        in_specs=[in_vmem, [in_vmem] * len(pieces)] + [in_vmem] * 3 + [from_hbm] * 4,
+        in_specs=[in_vmem, [in_vmem] * len(pieces)]
+        + [in_vmem] * 4
+        + [from_hbm] * 2
+        + [in_vmem],
         out_specs=(in_vmem,) * 3,
         scratch_shapes=[
             pltpu.VMEM((rows, group, head_dim), F32),
@@ -304,11 +312,9 @@
             pltpu.VMEM((rows, group, 1), F32),
             pltpu.VMEM((rows, group, head_dim), F32),
             pltpu.VMEM(cum.shape, BF16),
-            pltpu.VMEM(cum.shape, F32),
             pltpu.VMEM(keys.shape, BF16),
             pltpu.VMEM(values.shape, BF16),
-            pltpu.VMEM(out_w.shape, BF16),
-            pltpu.SemaphoreType.DMA((4, parts)),
+            pltpu.SemaphoreType.DMA((2, parts)),
         ],
         compiler_params=pltpu.CompilerParams(vmem_limit_bytes=24 * 2**20),
         cost_estimate=pl.CostEstimate(
@@ -316,7 +322,7 @@
             bytes_accessed=4 * keys.size + 4 * cum.size + 2 * out_w.size,
             transcendentals=cum.size,
         ),
-    )(own, pieces, scale, gate, lengths, *in_hbm(cum, keys, values, out_w))
+    )(own, pieces, scale, gate, lengths, cum, *in_hbm(keys, values), out_w)
 
 
 def cut_kernel(nz, nx, *refs):
@@ -440,7 +446,14 @@
     )
     logits = logits + bias_ref[...]
     gate = jnp.minimum(logits, 0.0) - jnp.log1p(jnp.exp(-jnp.abs(logits)))
-    log_gate_ref[...] = gate
+    across = lax.dot_general(
+        forget_ref[...], normed, (((1,), (1,)), ((), ())), preferred_element_type=F32
+    )
+    one = lax.broadcasted_iota(jnp.int32, (group, group), 0) == lax.broadcasted_iota(
+        jnp.int32, (group, group), 1
+    )
+    across = across + jnp.sum(jnp.where(one, bias_ref[...], 0.0), axis=1, keepdims=True)
+    log_gate_ref[...] = jnp.minimum(across, 0.0) - jnp.log1p(jnp.exp(-jnp.abs(across)))
     same = lax.broadcasted_iota(jnp.int32, (rows, group, group), 1) == lax.broadcasted_iota(
         jnp.int32, (rows, group, group), 2
     )
@@ -484,7 +497,7 @@
         functools.partial(early_kernel, len(arrays)),
         out_shape=(
             jax.ShapeDtypeStruct((rows, 1), F32),
-            jax.ShapeDtypeStruct((rows, group), F32),
+            jax.ShapeDtypeStruct((group, rows), F32),
             jax.ShapeDtypeStruct((rows, group, 1), F32),
             jax.ShapeDtypeStruct((rows, group, 1), jnp.int32),
             jax.ShapeDtypeStruct((slots, rows), BF16),
@@ -544,16 +557,18 @@
     own_partial, *partials = multiply([mine[0]] + moved, same_core, other_core)
     pieces = [shifted(partials[s - 1], "x", nx - s) for s in range(1, nx)]
 
+    logcum, out_rows = load(cache_logcum, w_out)
+
     partial_mix, new_keys, new_values = attend(
         own_partial,
         pieces,
         scale_attn,
         gate,
         long,
-        cache_logcum,
+        logcum,
         cache_keys,
         cache_values,
-        w_out,
+        out_rows,
     )
 
     mixes = [partial_mix] + [shifted(partial_mix, "y", s) for s in range(1, ny)]
@@ -575,7 +590,7 @@
         weighing, returned.astype(F32), (((0,), (0,)), ((), ())), preferred_element_type=F32
     )
     layer_out = (residual_cols + routed).astype(BF16)
-    return (layer_out, new_keys, new_values, new_log_gate)
+    return (layer_out, new_keys, new_values, new_log_gate.T)
 
 
 def solution(mesh):

time: 126 us -> 124 us (0.984)
  blocking collectives: 37.8 us -> 52.3 us
  waiting for transfers between devices: 37.6 us -> 27.6 us
  starting transfers between devices: 31.4 us -> 24.6 us
  Pallas kernels: 15.3 us -> 16.8 us
    all_to_all x2 -> x3, blocking collectives: 37.8 us -> 52.3 us  [exchange(): return lax.all_to_all(blocks, axis, split_axis=0, concat_axis=0, tiled=True)]
    all_to_all x3 -> x2, waiting for transfers between devices: 28.3 us -> 20.4 us  [exchange(): return lax.all_to_all(blocks, axis, split_axis=0, concat_axis=0, tiled=True)]
    all_to_all x3 -> x2, starting transfers between devices: 16.3 us -> 9.53 us  [exchange(): return lax.all_to_all(blocks, axis, split_axis=0, concat_axis=0, tiled=True)]
    ppermute x13, waiting for transfers between devices: 9.29 us -> 7.23 us  [shifted(): return lax.ppermute(value, axis, [(i, (i + step) % n) for i in range(n)])]
    pallas_call x0 -> x1, Pallas kernels: none -> 1.94 us  [load(): pl.pallas_call(functools.partial(load_kernel, len(arrays)), out_shape=[ja...]
  transfers between devices with their start and end apart: 16 -> 15, of which waited for: 9 -> 8; matrix products, arithmetic and copies ran while one was open for 1% -> 1% of each run, Pallas kernels for 2% -> 4%
where the time goes in v3:
time: 124 us
  blocking collectives  52.3 us (42%)
  waiting for transfers between devices  27.6 us (22%)
  starting transfers between devices  24.6 us (20%)
  Pallas kernels  16.8 us (14%)
    all_to_all x3, blocking collectives, exchange(): return lax.all_to_all(blocks, axis, split_axis=0, concat_axis=0, tiled=True)  52.3 us
    all_to_all x2, waiting for transfers between devices, exchange(): return lax.all_to_all(blocks, axis, split_axis=0, concat_axis=0, tiled=True)  20.4 us
    ppermute x13, starting transfers between devices, shifted(): return lax.ppermute(value, axis, [(i, (i + step) % n) for i in range(n)])  15.1 us
    all_to_all x2, starting transfers between devices, exchange(): return lax.all_to_all(blocks, axis, split_axis=0, concat_axis=0, tiled=True)  9.53 us
    ppermute x13, waiting for transfers between devices, shifted(): return lax.ppermute(value, axis, [(i, (i + step) % n) for i in range(n)])  7.23 us
    pallas_call x1, Pallas kernels, attend(): pl.pallas_call(functools.partial(attend_kernel, together, parts), out_sha...  5.44 us
    pallas_call x1, Pallas kernels, expert_rows(): pl.pallas_call(functools.partial(expert_kernel, nx), out_shape=jax.ShapeD...  4.04 us
  transfers between devices with their start and end apart: 15, of which 8 were waited for; matrix products, arithmetic and copies ran while one was open for 1% of the time, Pallas kernels for 4%

profile of v3, /device:TPU:8, one launch (start us, length us, event | category | flops | bytes accessed | tf_op | source)
XLA Modules:
  0.0 124.0 jit_solution(11802501569392180726)
XLA Ops:
  0.6 0.9 shard_map.211
  1.5 21.5 %all_to_all.25.refs_4_ = bf16[8,32,640]{2,1,0:T(8,128)(2,1)S(1)} all-to-all(bf16[8,32,640]{2,1,0:T(8,128)(2,1)S(1)} %shard_map.211), channel_id=1, replica_groups=mesh['z'=8,'x'=4,'c'=2,'y'=4] {'z'}, dimensions={0} | all-to-all | bytes 655360 | tf_op jit(solution)/shard_map/all_to_all | solution.py:27
  23.1 1.1 shard_map.210
  24.1 1.6 %collective-permute-start = (bf16[32,512]{1,0:T(8,128)(2,1)S(1)}, bf16[32,512]{1,0:T(8,128)(2,1)S(1)}, u32[]{:S(2)}, u32[]{:S(2)}) collective-permute-start(bf16[32,512]{1,0:T(8,128)(2,1)S(1)} %get-tuple-element.28), channel_id=1, source_target_pairs={{0,8},{8,16},{16,24},{24,0},{1,9},{9,17},{17,25},{25,1},{2,10},{10... | collective-permute-start | bytes 98312 | tf_op jit(solution)/shard_map/ppermute | solution.py:23
  25.7 2.7 %collective-permute-start.1 = (bf16[32,512]{1,0:T(8,128)(2,1)S(1)}, bf16[32,512]{1,0:T(8,128)(2,1)S(1)}, u32[]{:S(2)}, u32[]{:S(2)}) collective-permute-start(bf16[32,512]{1,0:T(8,128)(2,1)S(1)} %get-tuple-element.29), channel_id=1, source_target_pairs={{0,16},{8,24},{16,0},{24,8},{1,17},{9,25},{17,1},{25,9},{2,18},{10... | collective-permute-start | bytes 98312 | tf_op jit(solution)/shard_map/ppermute | solution.py:23
  28.4 1.4 %collective-permute-start.2 = (bf16[32,512]{1,0:T(8,128)(2,1)S(1)}, bf16[32,512]{1,0:T(8,128)(2,1)S(1)}, u32[]{:S(2)}, u32[]{:S(2)}) collective-permute-start(bf16[32,512]{1,0:T(8,128)(2,1)S(1)} %get-tuple-element.30), channel_id=1, source_target_pairs={{0,24},{8,0},{16,8},{24,16},{1,25},{9,1},{17,9},{25,17},{2,26},{10... | collective-permute-start | bytes 98312 | tf_op jit(solution)/shard_map/ppermute | solution.py:23
  29.9 1.3 %collective-permute-done.1.refs_2_ = bf16[32,512]{1,0:T(8,128)(2,1)S(1)} collective-permute-done((bf16[32,512]{1,0:T(8,128)(2,1)S(1)}, bf16[32,512]{1,0:T(8,128)(2,1)S(1)}, u32[]{:S(2)}, u32[]{:S(2)}) %collective-permute-start.1) | collective-permute-done | bytes 32800 | tf_op jit(solution)/shard_map/ppermute | solution.py:23
  31.1 1.2 collective-permute-done.2.refs_3_
  32.4 0.3 shard_map.212
  32.6 2.7 %collective-permute-start.4 = (bf16[32,640]{1,0:T(8,128)(2,1)S(1)}, bf16[32,640]{1,0:T(8,128)(2,1)S(1)}, u32[]{:S(2)}, u32[]{:S(2)}) collective-permute-start(bf16[32,640]{1,0:T(8,128)(2,1)S(1)} %get-tuple-element.32), channel_id=1, source_target_pairs={{0,24},{8,0},{16,8},{24,16},{1,25},{9,1},{17,9},{25,17},{2,26},{10... | collective-permute-start | bytes 122888 | tf_op jit(solution)/shard_map/ppermute | solution.py:23
  35.4 1.0 collective-permute-start.6
  36.3 1.9 %shard_map.214 = (f32[32,8,1024]{2,1,0:T(8,128)S(1)}, bf16[512,2048]{1,0:T(8,128)(2,1)S(1)}) custom-call(f32[32,8,1024]{2,1,0:T(8,128)} %refs_0_.5, bf16[512,2048]{1,0:T(8,128)(2,1)} %refs_1_.1), custom_call_target="tpu_custom_call" | custom-call | tf_op jit(solution)/shard_map/pallas_call | solution.py:284
  38.3 2.0 %shard_map.213 = (f32[32,1]{1,0:T(8,128)S(1)}, f32[8,32]{1,0:T(8,128)}, f32[32,8,1]{2,1,0:T(8,128)S(1)}, s32[32,8,1]{2,1,0:T(8,128)S(1)}, bf16[128,32]{1,0:T(8,1...) custom-call(bf16[32,2048]{1,0:T(8,128)(2,1)} %refs_0_.4, ...), custom_call_target="tpu_custom_call" | custom-call | tf_op jit(solution)/shard_map/pallas_call | solution.py:496
  40.2 0.7 collective-permute-done.5.pieces_refs_1_
  41.0 5.4 %shard_map.215 = (bf16[32,2048]{1,0:T(8,128)(2,1)S(1)}, bf16[32,64]{1,0:T(8,128)(2,1)}, bf16[32,64]{1,0:T(8,128)(2,1)}) custom-call(f32[32,640]{1,0:T(8,128)S(1)} %get-tuple-element.31.own_ref, bf16[32,640]{1,0:T(8,128)(2,1)S(1)} %collective-permute-done.4.pieces_refs_0_, bf16[32,640]{1,0:T(8,128)(2,1)S(1)} %collective-permute-done.5.pieces_refs_1_, ...), custom_call_target="tpu_custom_call" | custom-call | flops 134217728 | bytes 11534336 | tf_op jit(solution)/shard_map/pallas_call | solution.py:301
  46.5 1.7 %collective-permute-start.7 = (bf16[32,2048]{1,0:T(8,128)(2,1)S(1)}, bf16[32,2048]{1,0:T(8,128)(2,1)S(1)}, u32[]{:S(2)}, u32[]{:S(2)}) collective-permute-start(bf16[32,2048]{1,0:T(8,128)(2,1)S(1)} %get-tuple-element.40.mix_refs_0_), channel_id=1, source_target_pairs={{0,1},{1,2},{2,3},{3,0},{4,5},{5,6},{6,7},{7,4},{8,9},{9,10},{10,1... | collective-permute-start | bytes 393224 | tf_op jit(solution)/shard_map/ppermute | solution.py:23
  48.1 0.9 collective-permute-start.8
  49.1 2.4 %collective-permute-start.9 = (bf16[32,2048]{1,0:T(8,128)(2,1)S(1)}, bf16[32,2048]{1,0:T(8,128)(2,1)S(1)}, u32[]{:S(2)}, u32[]{:S(2)}) collective-permute-start(bf16[32,2048]{1,0:T(8,128)(2,1)S(1)} %get-tuple-element.40.mix_refs_0_), channel_id=1, source_target_pairs={{0,3},{1,0},{2,1},{3,2},{4,7},{5,4},{6,5},{7,6},{8,11},{9,8},{10,9... | collective-permute-start | bytes 393224 | tf_op jit(solution)/shard_map/ppermute | solution.py:23
  51.5 0.6 collective-permute-done.7.mix_refs_1_
  52.1 2.6 %collective-permute-done.8.mix_refs_2_ = bf16[32,2048]{1,0:T(8,128)(2,1)S(1)} collective-permute-done((bf16[32,2048]{1,0:T(8,128)(2,1)S(1)}, bf16[32,2048]{1,0:T(8,128)(2,1)S(1)}, u32[]{:S(2)}, u32[]{:S(2)}) %collective-permute-start.8) | collective-permute-done | bytes 131104 | tf_op jit(solution)/shard_map/ppermute | solution.py:23
  54.7 0.7 collective-permute-done.9.mix_refs_3_
  55.4 1.1 shard_map.216
  56.5 3.4 %all-to-all-start.1 = ((bf16[8,16,512]{2,1,0:T(8,128)(2,1)}), bf16[8,16,512]{2,1,0:T(8,128)(2,1)S(1)}, u32[]{:S(2)}, u32[]{:S(2)}) async-start(bf16[8,16,512]{2,1,0:T(8,128)(2,1)} %bitcast.8), calls=%async_computation.1 | async-start | bytes 262144 | tf_op jit(solution)/shard_map/all_to_all | solution.py:27
  60.0 0.5 collective-permute-start.11
  60.6 8.3 %all-to-all-done.1 = bf16[8,16,512]{2,1,0:T(8,128)(2,1)S(1)} async-done(((bf16[8,16,512]{2,1,0:T(8,128)(2,1)}), bf16[8,16,512]{2,1,0:T(8,128)(2,1)S(1)}, u32[]{:S(2)}, u32[]{:S(2)}) %all-to-all-start.1) | async-done | bytes 131104 | tf_op jit(solution)/shard_map/all_to_all | solution.py:27
  68.9 1.1 broadcast_in_dim.8
  70.0 6.2 %all-to-all-start.2 = ((bf16[16,64,512]{2,1,0:T(8,128)(2,1)}), bf16[16,64,512]{2,1,0:T(8,128)(2,1)S(1)}, u32[]{:S(2)}, u32[]{:S(2)}) async-start(bf16[16,64,512]{2,1,0:T(8,128)(2,1)} %bitcast.21), calls=%async_computation.2 | async-start | bytes 2097152 | tf_op jit(solution)/shard_map/all_to_all | solution.py:27
  76.2 12.1 %all-to-all-done.2.rows_ref = bf16[16,64,512]{2,1,0:T(8,128)(2,1)S(1)} async-done(((bf16[16,64,512]{2,1,0:T(8,128)(2,1)}), bf16[16,64,512]{2,1,0:T(8,128)(2,1)S(1)}, u32[]{:S(2)}, u32[]{:S(2)}) %all-to-all-start.2) | async-done | bytes 1048608 | tf_op jit(solution)/shard_map/all_to_all | solution.py:27
  88.3 4.0 %shard_map.217 = bf16[16,64,512]{2,1,0:T(8,128)(2,1)S(1)} custom-call(bf16[16,64,512]{2,1,0:T(8,128)(2,1)S(1)} %all-to-all-done.2.rows_ref, bf16[2048,256]{1,0:T(8,128)(2,1)S(1)} %copy-done, bf16[2048,256]{1,0:T(8,128)(2,1)} %collective-permute-done.10.gate_refs_1_, bf16[2048,256]{1,0:T(8,128)(2,1)S(1)} %copy-done.1, ...), custom_call_target="tpu_custom_call" | custom-call | flops 1610612736 | bytes 8388608 | tf_op jit(solution)/shard_map/pallas_call | solution.py:58
  92.3 16.2 %all_to_all.26.partials_ref = bf16[16,64,512]{2,1,0:T(8,128)(2,1)S(1)} all-to-all(bf16[16,64,512]{2,1,0:T(8,128)(2,1)S(1)} %shard_map.217), channel_id=1, replica_groups=mesh['z'=8,'x'=4,'c'=2,'y'=4] {'x','y'}, dimensions={0} | all-to-all | bytes 2097152 | tf_op jit(solution)/shard_map/all_to_all | solution.py:27
  108.7 14.5 %all_to_all.27 = bf16[8,16,512]{2,1,0:T(8,128)(2,1)S(1)} all-to-all(bf16[8,16,512]{2,1,0:T(8,128)(2,1)S(1)} %shard_map.218), channel_id=1, replica_groups=mesh['z'=8,'x'=4,'c'=2,'y'=4] {'z'}, dimensions={0} | all-to-all | bytes 262144 | tf_op jit(solution)/shard_map/all_to_all | solution.py:27
  123.4 0.6 add_convert_fusion
  (18 shorter events, 0.6 us)
Async XLA Ops:
  23.1 9.3 %collective-permute-start.3 = (bf16[8,32,640]{2,1,0:T(8,128)(2,1)S(1)}, bf16[8,32,640]{2,1,0:T(8,128)(2,1)S(1)}, u32[]{:S(2)}, u32[]{:S(2)}) collective-permute-start(bf16[8,32,640]{2,1,0:T(8,128)(2,1)S(1)} %all_to_all.25.refs_4_), channel_id=1, source_target_pairs={{0,4},{4,0},{1,5},{5,1},{2,6},{6,2},{3,7},{7,3},{8,12},{12,8},{9,1... | collective-permute-start | bytes 983048 | tf_op jit(solution)/shard_map/ppermute | solution.py:23
  24.1 5.7 %collective-permute-start = (bf16[32,512]{1,0:T(8,128)(2,1)S(1)}, bf16[32,512]{1,0:T(8,128)(2,1)S(1)}, u32[]{:S(2)}, u32[]{:S(2)}) collective-permute-start(bf16[32,512]{1,0:T(8,128)(2,1)S(1)} %get-tuple-element.28), channel_id=1, source_target_pairs={{0,8},{8,16},{16,24},{24,0},{1,9},{9,17},{17,25},{25,1},{2,10},{10... | collective-permute-start | bytes 98312 | tf_op jit(solution)/shard_map/ppermute | solution.py:23
  25.7 5.4 %collective-permute-start.1 = (bf16[32,512]{1,0:T(8,128)(2,1)S(1)}, bf16[32,512]{1,0:T(8,128)(2,1)S(1)}, u32[]{:S(2)}, u32[]{:S(2)}) collective-permute-start(bf16[32,512]{1,0:T(8,128)(2,1)S(1)} %get-tuple-element.29), channel_id=1, source_target_pairs={{0,16},{8,24},{16,0},{24,8},{1,17},{9,25},{17,1},{25,9},{2,18},{10... | collective-permute-start | bytes 98312 | tf_op jit(solution)/shard_map/ppermute | solution.py:23
  28.4 3.9 %collective-permute-start.2 = (bf16[32,512]{1,0:T(8,128)(2,1)S(1)}, bf16[32,512]{1,0:T(8,128)(2,1)S(1)}, u32[]{:S(2)}, u32[]{:S(2)}) collective-permute-start(bf16[32,512]{1,0:T(8,128)(2,1)S(1)} %get-tuple-element.30), channel_id=1, source_target_pairs={{0,24},{8,0},{16,8},{24,16},{1,25},{9,1},{17,9},{25,17},{2,26},{10... | collective-permute-start | bytes 98312 | tf_op jit(solution)/shard_map/ppermute | solution.py:23
  32.6 7.6 %collective-permute-start.4 = (bf16[32,640]{1,0:T(8,128)(2,1)S(1)}, bf16[32,640]{1,0:T(8,128)(2,1)S(1)}, u32[]{:S(2)}, u32[]{:S(2)}) collective-permute-start(bf16[32,640]{1,0:T(8,128)(2,1)S(1)} %get-tuple-element.32), channel_id=1, source_target_pairs={{0,24},{8,0},{16,8},{24,16},{1,25},{9,1},{17,9},{25,17},{2,26},{10... | collective-permute-start | bytes 122888 | tf_op jit(solution)/shard_map/ppermute | solution.py:23
  35.4 5.6 %collective-permute-start.5 = (bf16[32,640]{1,0:T(8,128)(2,1)S(1)}, bf16[32,640]{1,0:T(8,128)(2,1)S(1)}, u32[]{:S(2)}, u32[]{:S(2)}) collective-permute-start(bf16[32,640]{1,0:T(8,128)(2,1)S(1)} %get-tuple-element.33), channel_id=1, source_target_pairs={{0,16},{8,24},{16,0},{24,8},{1,17},{9,25},{17,1},{25,9},{2,18},{10... | collective-permute-start | bytes 122888 | tf_op jit(solution)/shard_map/ppermute | solution.py:23
  35.4 5.7 %collective-permute-start.6 = (bf16[32,640]{1,0:T(8,128)(2,1)S(1)}, bf16[32,640]{1,0:T(8,128)(2,1)S(1)}, u32[]{:S(2)}, u32[]{:S(2)}) collective-permute-start(bf16[32,640]{1,0:T(8,128)(2,1)S(1)} %get-tuple-element.34), channel_id=1, source_target_pairs={{0,8},{8,16},{16,24},{24,0},{1,9},{9,17},{17,25},{25,1},{2,10},{10... | collective-permute-start | bytes 122888 | tf_op jit(solution)/shard_map/ppermute | solution.py:23
  41.0 18.9 %copy-start = (bf16[2048,256]{1,0:T(8,128)(2,1)S(1)}, bf16[2048,256]{1,0:T(8,128)(2,1)}, u32[]{:S(2)}) copy-start(bf16[2048,256]{1,0:T(8,128)(2,1)} %gate_refs_0_.1) | copy-start | bytes 3145732
  41.0 19.0 %copy-start.1 = (bf16[2048,256]{1,0:T(8,128)(2,1)S(1)}, bf16[2048,256]{1,0:T(8,128)(2,1)}, u32[]{:S(2)}) copy-start(bf16[2048,256]{1,0:T(8,128)(2,1)} %up_refs_0_.1) | copy-start | bytes 3145732
  46.5 5.6 %collective-permute-start.7 = (bf16[32,2048]{1,0:T(8,128)(2,1)S(1)}, bf16[32,2048]{1,0:T(8,128)(2,1)S(1)}, u32[]{:S(2)}, u32[]{:S(2)}) collective-permute-start(bf16[32,2048]{1,0:T(8,128)(2,1)S(1)} %get-tuple-element.40.mix_refs_0_), channel_id=1, source_target_pairs={{0,1},{1,2},{2,3},{3,0},{4,5},{5,6},{6,7},{7,4},{8,9},{9,10},{10,1... | collective-permute-start | bytes 393224 | tf_op jit(solution)/shard_map/ppermute | solution.py:23
  48.1 6.6 %collective-permute-start.8 = (bf16[32,2048]{1,0:T(8,128)(2,1)S(1)}, bf16[32,2048]{1,0:T(8,128)(2,1)S(1)}, u32[]{:S(2)}, u32[]{:S(2)}) collective-permute-start(bf16[32,2048]{1,0:T(8,128)(2,1)S(1)} %get-tuple-element.40.mix_refs_0_), channel_id=1, source_target_pairs={{0,2},{1,3},{2,0},{3,1},{4,6},{5,7},{6,4},{7,5},{8,10},{9,11},{10,... | collective-permute-start | bytes 393224 | tf_op jit(solution)/shard_map/ppermute | solution.py:23
  49.1 6.4 %collective-permute-start.9 = (bf16[32,2048]{1,0:T(8,128)(2,1)S(1)}, bf16[32,2048]{1,0:T(8,128)(2,1)S(1)}, u32[]{:S(2)}, u32[]{:S(2)}) collective-permute-start(bf16[32,2048]{1,0:T(8,128)(2,1)S(1)} %get-tuple-element.40.mix_refs_0_), channel_id=1, source_target_pairs={{0,3},{1,0},{2,1},{3,2},{4,7},{5,4},{6,5},{7,6},{8,11},{9,8},{10,9... | collective-permute-start | bytes 393224 | tf_op jit(solution)/shard_map/ppermute | solution.py:23
  56.5 12.4 %all-to-all-start.1 = ((bf16[8,16,512]{2,1,0:T(8,128)(2,1)}), bf16[8,16,512]{2,1,0:T(8,128)(2,1)S(1)}, u32[]{:S(2)}, u32[]{:S(2)}) async-start(bf16[8,16,512]{2,1,0:T(8,128)(2,1)} %bitcast.8), calls=%async_computation.1 | async-start | bytes 262144 | tf_op jit(solution)/shard_map/all_to_all | solution.py:27
  59.9 16.2 %collective-permute-start.10 = (bf16[2048,256]{1,0:T(8,128)(2,1)S(1)}, bf16[2048,256]{1,0:T(8,128)(2,1)}, u32[]{:S(2)}, u32[]{:S(2)}) collective-permute-start(bf16[2048,256]{1,0:T(8,128)(2,1)S(1)} %copy-done), channel_id=1, source_target_pairs={{0,4},{4,0},{1,5},{5,1},{2,6},{6,2},{3,7},{7,3},{8,12},{12,8},{9,1... | collective-permute-start | bytes 3145736 | tf_op jit(solution)/shard_map/ppermute | solution.py:23
  60.0 16.1 %collective-permute-start.11 = (bf16[2048,256]{1,0:T(8,128)(2,1)S(1)}, bf16[2048,256]{1,0:T(8,128)(2,1)}, u32[]{:S(2)}, u32[]{:S(2)}) collective-permute-start(bf16[2048,256]{1,0:T(8,128)(2,1)S(1)} %copy-done.1), channel_id=1, source_target_pairs={{0,4},{4,0},{1,5},{5,1},{2,6},{6,2},{3,7},{7,3},{8,12},{12,8},{9,1... | collective-permute-start | bytes 3145736 | tf_op jit(solution)/shard_map/ppermute | solution.py:23
  60.5 15.7 %collective-permute-start.12 = (bf16[256,2048]{1,0:T(8,128)(2,1)}, bf16[256,2048]{1,0:T(8,128)(2,1)}, u32[]{:S(2)}, u32[]{:S(2)}) collective-permute-start(bf16[256,2048]{1,0:T(8,128)(2,1)} %down_refs_0_.1), channel_id=1, source_target_pairs={{0,4},{4,0},{1,5},{5,1},{2,6},{6,2},{3,7},{7,3},{8,12},{12,8},{9,1... | collective-permute-start | bytes 3145736 | tf_op jit(solution)/shard_map/ppermute | solution.py:23
  70.0 18.3 %all-to-all-start.2 = ((bf16[16,64,512]{2,1,0:T(8,128)(2,1)}), bf16[16,64,512]{2,1,0:T(8,128)(2,1)S(1)}, u32[]{:S(2)}, u32[]{:S(2)}) async-start(bf16[16,64,512]{2,1,0:T(8,128)(2,1)} %bitcast.21), calls=%async_computation.2 | async-start | bytes 2097152 | tf_op jit(solution)/shard_map/all_to_all | solution.py:27

commit v4 on v3

--- a/solution.py
+++ b/solution.py
@@ -158,6 +158,7 @@
     gate_ref,
     length_ref,
     cum_ref,
+    early_keys_ref,
     keys_ref,
     values_ref,
     out_w_ref,
@@ -171,6 +172,7 @@
     past_s,
     keys_s,
     values_s,
+    out_w_s,
     sems,
 ):
     rows, group, head_dim = q_s.shape
@@ -186,10 +188,14 @@
             for p, h in enumerate(halves)
         ]
 
-    key_copies = copies(0, keys_ref, keys_s)
+    late = halves[1]
+    key_copy = pltpu.make_async_copy(keys_ref.at[late], keys_s, sems.at[0, 0])
+    out_w_copy = pltpu.make_async_copy(out_w_ref, out_w_s, sems.at[0, 1])
     value_copies = copies(1, values_ref, values_s)
-    for copy in key_copies + value_copies:
+    key_copy.start()
+    for copy in value_copies:
         copy.start()
+    out_w_copy.start()
 
     projected = own_ref[...]
     for ref in pieces_refs:
@@ -222,7 +228,12 @@
 
     def weigh(some):
         scores = [
-            jnp.dot(q_s[b].astype(BF16), keys_s[b], preferred_element_type=F32) * scale
+            jnp.dot(
+                q_s[b].astype(BF16),
+                early_keys_ref[b] if b < share else keys_s[b - share],
+                preferred_element_type=F32,
+            )
+            * scale
             for b in some
         ]
         lengths = [length_ref[b] for b in some]
@@ -261,7 +272,8 @@
             heads_s[b] = one
 
     for p in range(parts):
-        key_copies[p].wait()
+        if p > 0:
+            key_copy.wait()
         for first in range(p * share, (p + 1) * share, together):
             weigh(range(first, first + together))
     for p in range(parts):
@@ -273,17 +285,25 @@
     wide = lax.dot_general(heads, fold, (((1,), (1,)), ((), ())), preferred_element_type=F32)
     wide = jnp.where(on_head, wide.reshape(rows, group, cols), 0.0)
     heads_out = jnp.sum(wide, axis=1).astype(BF16)
-    mix_ref[...] = jnp.dot(heads_out, out_w_ref[...], preferred_element_type=F32).astype(BF16)
+    out_w_copy.wait()
+    mix_ref[...] = jnp.dot(heads_out, out_w_s[...], preferred_element_type=F32).astype(BF16)
 
 
 def load_kernel(count, *refs):
-    fetched(refs[:count], refs[count:-1], refs[-1])
-
-
-def load(*arrays):
+    sources, targets = refs[:count], refs[count:-1]
+    sources = [
+        source.at[pl.ds(0, target.shape[0])] for source, target in zip(sources, targets)
+    ]
+    fetched(sources, targets, refs[-1])
+
+
+def load(arrays, heights):
     return pl.pallas_call(
         functools.partial(load_kernel, len(arrays)),
-        out_shape=[jax.ShapeDtypeStruct(array.shape, array.dtype) for array in arrays],
+        out_shape=[
+            jax.ShapeDtypeStruct((height, *array.shape[1:]), array.dtype)
+            for array, height in zip(arrays, heights)
+        ],
         in_specs=[pl.BlockSpec(memory_space=pltpu.HBM)] * len(arrays),
         out_specs=[pl.BlockSpec(memory_space=pltpu.VMEM)] * len(arrays),
         scratch_shapes=[pltpu.SemaphoreType.DMA((len(arrays),))],
@@ -291,7 +311,7 @@
     )(*in_hbm(*arrays))
 
 
-def attend(own, pieces, scale, gate, lengths, cum, keys, values, out_w):
+def attend(own, pieces, scale, gate, lengths, cum, early_keys, keys, values, out_w):
     rows, group, _ = cum.shape
     head_dim, width = keys.shape[1], out_w.shape[1]
     in_vmem = pl.BlockSpec(memory_space=pltpu.VMEM)
@@ -302,9 +322,8 @@
         functools.partial(attend_kernel, together, parts),
         out_shape=(jax.ShapeDtypeStruct((rows, width), BF16), one, one),
         in_specs=[in_vmem, [in_vmem] * len(pieces)]
-        + [in_vmem] * 4
-        + [from_hbm] * 2
-        + [in_vmem],
+        + [in_vmem] * 5
+        + [from_hbm] * 3,
         out_specs=(in_vmem,) * 3,
         scratch_shapes=[
             pltpu.VMEM((rows, group, head_dim), F32),
@@ -312,8 +331,9 @@
             pltpu.VMEM((rows, group, 1), F32),
             pltpu.VMEM((rows, group, head_dim), F32),
             pltpu.VMEM(cum.shape, BF16),
-            pltpu.VMEM(keys.shape, BF16),
+            pltpu.VMEM((rows // parts, *keys.shape[1:]), BF16),
             pltpu.VMEM(values.shape, BF16),
+            pltpu.VMEM(out_w.shape, BF16),
             pltpu.SemaphoreType.DMA((2, parts)),
         ],
         compiler_params=pltpu.CompilerParams(vmem_limit_bytes=24 * 2**20),
@@ -322,7 +342,7 @@
             bytes_accessed=4 * keys.size + 4 * cum.size + 2 * out_w.size,
             transcendentals=cum.size,
         ),
-    )(own, pieces, scale, gate, lengths, cum, *in_hbm(keys, values), out_w)
+    )(own, pieces, scale, gate, lengths, cum, early_keys, *in_hbm(keys, values, out_w))
 
 
 def cut_kernel(nz, nx, *refs):
@@ -533,7 +553,7 @@
     routes,
     route_weights,
 ):
-    _, width = tokens.shape
+    rows, width = tokens.shape
     nz, nx, _, ny = (lax.axis_size(a) for a in ("z", "x", "c", "y"))
 
     scale_attn, new_log_gate, gate, long, selector, weighing, kept, gains = early(
@@ -557,7 +577,7 @@
     own_partial, *partials = multiply([mine[0]] + moved, same_core, other_core)
     pieces = [shifted(partials[s - 1], "x", nx - s) for s in range(1, nx)]
 
-    logcum, out_rows = load(cache_logcum, w_out)
+    logcum, early_keys = load((cache_logcum, cache_keys), (rows, rows // 2))
 
     partial_mix, new_keys, new_values = attend(
         own_partial,
@@ -566,9 +586,10 @@
         gate,
         long,
         logcum,
+        early_keys,
         cache_keys,
         cache_values,
-        out_rows,
+        w_out,
     )
 
     mixes = [partial_mix] + [shifted(partial_mix, "y", s) for s in range(1, ny)]

time: 124 us -> 124 us (level)
  no operation moved by 1% of the time
where the time goes in v4:
time: 124 us; the launch traced here: 123 us
  blocking collectives  52.3 us (42%)
  waiting for transfers between devices  27.6 us (22%)
  starting transfers between devices  24.6 us (20%)
  Pallas kernels  16.1 us (13%)
    all_to_all x3, blocking collectives, exchange(): return lax.all_to_all(blocks, axis, split_axis=0, concat_axis=0, tiled=True)  52.3 us
    all_to_all x2, waiting for transfers between devices, exchange(): return lax.all_to_all(blocks, axis, split_axis=0, concat_axis=0, tiled=True)  20.4 us
    ppermute x13, starting transfers between devices, shifted(): return lax.ppermute(value, axis, [(i, (i + step) % n) for i in range(n)])  15.1 us
    all_to_all x2, starting transfers between devices, exchange(): return lax.all_to_all(blocks, axis, split_axis=0, concat_axis=0, tiled=True)  9.52 us
    ppermute x13, waiting for transfers between devices, shifted(): return lax.ppermute(value, axis, [(i, (i + step) % n) for i in range(n)])  7.24 us
    pallas_call x1, Pallas kernels, attend(): pl.pallas_call(functools.partial(attend_kernel, together, parts), out_sha...  4.75 us
    pallas_call x1, Pallas kernels, expert_rows(): pl.pallas_call(functools.partial(expert_kernel, nx), out_shape=jax.ShapeD...  4.04 us
  transfers between devices with their start and end apart: 15, of which 8 were waited for; matrix products, arithmetic and copies ran while one was open for 1% of the time, Pallas kernels for 4%

profile of v4, /device:TPU:8, one launch (start us, length us, event | category | flops | bytes accessed | tf_op | source)
XLA Modules:
  0.0 123.3 jit_solution(12104528207785074247)
XLA Ops:
  0.6 0.9 shard_map.211
  1.5 21.5 %all_to_all.25.refs_4_ = bf16[8,32,640]{2,1,0:T(8,128)(2,1)S(1)} all-to-all(bf16[8,32,640]{2,1,0:T(8,128)(2,1)S(1)} %shard_map.211), channel_id=1, replica_groups=mesh['z'=8,'x'=4,'c'=2,'y'=4] {'z'}, dimensions={0} | all-to-all | bytes 655360 | tf_op jit(solution)/shard_map/all_to_all | solution.py:27
  23.1 1.1 shard_map.210
  24.1 1.6 %collective-permute-start = (bf16[32,512]{1,0:T(8,128)(2,1)S(1)}, bf16[32,512]{1,0:T(8,128)(2,1)S(1)}, u32[]{:S(2)}, u32[]{:S(2)}) collective-permute-start(bf16[32,512]{1,0:T(8,128)(2,1)S(1)} %get-tuple-element.28), channel_id=1, source_target_pairs={{0,8},{8,16},{16,24},{24,0},{1,9},{9,17},{17,25},{25,1},{2,10},{10... | collective-permute-start | bytes 98312 | tf_op jit(solution)/shard_map/ppermute | solution.py:23
  25.7 2.7 %collective-permute-start.1 = (bf16[32,512]{1,0:T(8,128)(2,1)S(1)}, bf16[32,512]{1,0:T(8,128)(2,1)S(1)}, u32[]{:S(2)}, u32[]{:S(2)}) collective-permute-start(bf16[32,512]{1,0:T(8,128)(2,1)S(1)} %get-tuple-element.29), channel_id=1, source_target_pairs={{0,16},{8,24},{16,0},{24,8},{1,17},{9,25},{17,1},{25,9},{2,18},{10... | collective-permute-start | bytes 98312 | tf_op jit(solution)/shard_map/ppermute | solution.py:23
  28.4 1.4 %collective-permute-start.2 = (bf16[32,512]{1,0:T(8,128)(2,1)S(1)}, bf16[32,512]{1,0:T(8,128)(2,1)S(1)}, u32[]{:S(2)}, u32[]{:S(2)}) collective-permute-start(bf16[32,512]{1,0:T(8,128)(2,1)S(1)} %get-tuple-element.30), channel_id=1, source_target_pairs={{0,24},{8,0},{16,8},{24,16},{1,25},{9,1},{17,9},{25,17},{2,26},{10... | collective-permute-start | bytes 98312 | tf_op jit(solution)/shard_map/ppermute | solution.py:23
  29.9 1.3 %collective-permute-done.1.refs_2_ = bf16[32,512]{1,0:T(8,128)(2,1)S(1)} collective-permute-done((bf16[32,512]{1,0:T(8,128)(2,1)S(1)}, bf16[32,512]{1,0:T(8,128)(2,1)S(1)}, u32[]{:S(2)}, u32[]{:S(2)}) %collective-permute-start.1) | collective-permute-done | bytes 32800 | tf_op jit(solution)/shard_map/ppermute | solution.py:23
  31.1 1.2 collective-permute-done.2.refs_3_
  32.4 0.3 shard_map.212
  32.6 2.7 %collective-permute-start.4 = (bf16[32,640]{1,0:T(8,128)(2,1)S(1)}, bf16[32,640]{1,0:T(8,128)(2,1)S(1)}, u32[]{:S(2)}, u32[]{:S(2)}) collective-permute-start(bf16[32,640]{1,0:T(8,128)(2,1)S(1)} %get-tuple-element.32), channel_id=1, source_target_pairs={{0,24},{8,0},{16,8},{24,16},{1,25},{9,1},{17,9},{25,17},{2,26},{10... | collective-permute-start | bytes 122888 | tf_op jit(solution)/shard_map/ppermute | solution.py:23
  35.4 1.0 collective-permute-start.6
  36.3 1.9 %shard_map.214 = (f32[32,8,1024]{2,1,0:T(8,128)S(1)}, bf16[16,64,1024]{2,1,0:T(8,128)(2,1)S(1)}) custom-call(f32[32,8,1024]{2,1,0:T(8,128)} %refs_0_.5, bf16[32,64,1024]{2,1,0:T(8,128)(2,1)} %keys_ref.1), custom_call_target="tpu_custom_call" | custom-call | tf_op jit(solution)/shard_map/pallas_call | solution.py:301
  38.3 2.0 %shard_map.213 = (f32[32,1]{1,0:T(8,128)S(1)}, f32[8,32]{1,0:T(8,128)}, f32[32,8,1]{2,1,0:T(8,128)S(1)}, s32[32,8,1]{2,1,0:T(8,128)S(1)}, bf16[128,32]{1,0:T(8,1...) custom-call(bf16[32,2048]{1,0:T(8,128)(2,1)} %refs_0_.4, ...), custom_call_target="tpu_custom_call" | custom-call | tf_op jit(solution)/shard_map/pallas_call | solution.py:516
  40.2 0.7 collective-permute-done.5.pieces_refs_1_
  41.0 4.8 %shard_map.215 = (bf16[32,2048]{1,0:T(8,128)(2,1)S(1)}, bf16[32,64]{1,0:T(8,128)(2,1)}, bf16[32,64]{1,0:T(8,128)(2,1)}) custom-call(f32[32,640]{1,0:T(8,128)S(1)} %get-tuple-element.31.own_ref, bf16[32,640]{1,0:T(8,128)(2,1)S(1)} %collective-permute-done.4.pieces_refs_0_, bf16[32,640]{1,0:T(8,128)(2,1)S(1)} %collective-permute-done.5.pieces_refs_1_, ...), custom_call_target="tpu_custom_call" | custom-call | flops 134217728 | bytes 11534336 | tf_op jit(solution)/shard_map/pallas_call | solution.py:321
  45.8 1.7 %collective-permute-start.7 = (bf16[32,2048]{1,0:T(8,128)(2,1)S(1)}, bf16[32,2048]{1,0:T(8,128)(2,1)S(1)}, u32[]{:S(2)}, u32[]{:S(2)}) collective-permute-start(bf16[32,2048]{1,0:T(8,128)(2,1)S(1)} %get-tuple-element.40.mix_refs_0_), channel_id=1, source_target_pairs={{0,1},{1,2},{2,3},{3,0},{4,5},{5,6},{6,7},{7,4},{8,9},{9,10},{10,1... | collective-permute-start | bytes 393224 | tf_op jit(solution)/shard_map/ppermute | solution.py:23
  47.4 0.9 collective-permute-start.8
  48.4 2.4 %collective-permute-start.9 = (bf16[32,2048]{1,0:T(8,128)(2,1)S(1)}, bf16[32,2048]{1,0:T(8,128)(2,1)S(1)}, u32[]{:S(2)}, u32[]{:S(2)}) collective-permute-start(bf16[32,2048]{1,0:T(8,128)(2,1)S(1)} %get-tuple-element.40.mix_refs_0_), channel_id=1, source_target_pairs={{0,3},{1,0},{2,1},{3,2},{4,7},{5,4},{6,5},{7,6},{8,11},{9,8},{10,9... | collective-permute-start | bytes 393224 | tf_op jit(solution)/shard_map/ppermute | solution.py:23
  50.8 0.6 collective-permute-done.7.mix_refs_1_
  51.4 2.6 %collective-permute-done.8.mix_refs_2_ = bf16[32,2048]{1,0:T(8,128)(2,1)S(1)} collective-permute-done((bf16[32,2048]{1,0:T(8,128)(2,1)S(1)}, bf16[32,2048]{1,0:T(8,128)(2,1)S(1)}, u32[]{:S(2)}, u32[]{:S(2)}) %collective-permute-start.8) | collective-permute-done | bytes 131104 | tf_op jit(solution)/shard_map/ppermute | solution.py:23
  54.0 0.7 collective-permute-done.9.mix_refs_3_
  54.8 1.1 shard_map.216
  55.9 3.4 %all-to-all-start.1 = ((bf16[8,16,512]{2,1,0:T(8,128)(2,1)}), bf16[8,16,512]{2,1,0:T(8,128)(2,1)S(1)}, u32[]{:S(2)}, u32[]{:S(2)}) async-start(bf16[8,16,512]{2,1,0:T(8,128)(2,1)} %bitcast.8), calls=%async_computation.1 | async-start | bytes 262144 | tf_op jit(solution)/shard_map/all_to_all | solution.py:27
  59.4 0.5 collective-permute-start.11
  60.0 8.3 %all-to-all-done.1 = bf16[8,16,512]{2,1,0:T(8,128)(2,1)S(1)} async-done(((bf16[8,16,512]{2,1,0:T(8,128)(2,1)}), bf16[8,16,512]{2,1,0:T(8,128)(2,1)S(1)}, u32[]{:S(2)}, u32[]{:S(2)}) %all-to-all-start.1) | async-done | bytes 131104 | tf_op jit(solution)/shard_map/all_to_all | solution.py:27
  68.2 1.1 broadcast_in_dim.8
  69.3 6.2 %all-to-all-start.2 = ((bf16[16,64,512]{2,1,0:T(8,128)(2,1)}), bf16[16,64,512]{2,1,0:T(8,128)(2,1)S(1)}, u32[]{:S(2)}, u32[]{:S(2)}) async-start(bf16[16,64,512]{2,1,0:T(8,128)(2,1)} %bitcast.21), calls=%async_computation.2 | async-start | bytes 2097152 | tf_op jit(solution)/shard_map/all_to_all | solution.py:27
  75.5 12.1 %all-to-all-done.2.rows_ref = bf16[16,64,512]{2,1,0:T(8,128)(2,1)S(1)} async-done(((bf16[16,64,512]{2,1,0:T(8,128)(2,1)}), bf16[16,64,512]{2,1,0:T(8,128)(2,1)S(1)}, u32[]{:S(2)}, u32[]{:S(2)}) %all-to-all-start.2) | async-done | bytes 1048608 | tf_op jit(solution)/shard_map/all_to_all | solution.py:27
  87.6 4.0 %shard_map.217 = bf16[16,64,512]{2,1,0:T(8,128)(2,1)S(1)} custom-call(bf16[16,64,512]{2,1,0:T(8,128)(2,1)S(1)} %all-to-all-done.2.rows_ref, bf16[2048,256]{1,0:T(8,128)(2,1)S(1)} %copy-done, bf16[2048,256]{1,0:T(8,128)(2,1)} %collective-permute-done.10.gate_refs_1_, bf16[2048,256]{1,0:T(8,128)(2,1)S(1)} %copy-done.1, ...), custom_call_target="tpu_custom_call" | custom-call | flops 1610612736 | bytes 8388608 | tf_op jit(solution)/shard_map/pallas_call | solution.py:58
  91.6 16.2 %all_to_all.26.partials_ref = bf16[16,64,512]{2,1,0:T(8,128)(2,1)S(1)} all-to-all(bf16[16,64,512]{2,1,0:T(8,128)(2,1)S(1)} %shard_map.217), channel_id=1, replica_groups=mesh['z'=8,'x'=4,'c'=2,'y'=4] {'x','y'}, dimensions={0} | all-to-all | bytes 2097152 | tf_op jit(solution)/shard_map/all_to_all | solution.py:27
  108.0 14.5 %all_to_all.27 = bf16[8,16,512]{2,1,0:T(8,128)(2,1)S(1)} all-to-all(bf16[8,16,512]{2,1,0:T(8,128)(2,1)S(1)} %shard_map.218), channel_id=1, replica_groups=mesh['z'=8,'x'=4,'c'=2,'y'=4] {'z'}, dimensions={0} | all-to-all | bytes 262144 | tf_op jit(solution)/shard_map/all_to_all | solution.py:27
  122.7 0.6 add_convert_fusion
  (18 shorter events, 0.6 us)
Async XLA Ops:
  23.1 9.3 %collective-permute-start.3 = (bf16[8,32,640]{2,1,0:T(8,128)(2,1)S(1)}, bf16[8,32,640]{2,1,0:T(8,128)(2,1)S(1)}, u32[]{:S(2)}, u32[]{:S(2)}) collective-permute-start(bf16[8,32,640]{2,1,0:T(8,128)(2,1)S(1)} %all_to_all.25.refs_4_), channel_id=1, source_target_pairs={{0,4},{4,0},{1,5},{5,1},{2,6},{6,2},{3,7},{7,3},{8,12},{12,8},{9,1... | collective-permute-start | bytes 983048 | tf_op jit(solution)/shard_map/ppermute | solution.py:23
  24.1 5.7 %collective-permute-start = (bf16[32,512]{1,0:T(8,128)(2,1)S(1)}, bf16[32,512]{1,0:T(8,128)(2,1)S(1)}, u32[]{:S(2)}, u32[]{:S(2)}) collective-permute-start(bf16[32,512]{1,0:T(8,128)(2,1)S(1)} %get-tuple-element.28), channel_id=1, source_target_pairs={{0,8},{8,16},{16,24},{24,0},{1,9},{9,17},{17,25},{25,1},{2,10},{10... | collective-permute-start | bytes 98312 | tf_op jit(solution)/shard_map/ppermute | solution.py:23
  25.7 5.4 %collective-permute-start.1 = (bf16[32,512]{1,0:T(8,128)(2,1)S(1)}, bf16[32,512]{1,0:T(8,128)(2,1)S(1)}, u32[]{:S(2)}, u32[]{:S(2)}) collective-permute-start(bf16[32,512]{1,0:T(8,128)(2,1)S(1)} %get-tuple-element.29), channel_id=1, source_target_pairs={{0,16},{8,24},{16,0},{24,8},{1,17},{9,25},{17,1},{25,9},{2,18},{10... | collective-permute-start | bytes 98312 | tf_op jit(solution)/shard_map/ppermute | solution.py:23
  28.4 3.9 %collective-permute-start.2 = (bf16[32,512]{1,0:T(8,128)(2,1)S(1)}, bf16[32,512]{1,0:T(8,128)(2,1)S(1)}, u32[]{:S(2)}, u32[]{:S(2)}) collective-permute-start(bf16[32,512]{1,0:T(8,128)(2,1)S(1)} %get-tuple-element.30), channel_id=1, source_target_pairs={{0,24},{8,0},{16,8},{24,16},{1,25},{9,1},{17,9},{25,17},{2,26},{10... | collective-permute-start | bytes 98312 | tf_op jit(solution)/shard_map/ppermute | solution.py:23
  32.6 7.6 %collective-permute-start.4 = (bf16[32,640]{1,0:T(8,128)(2,1)S(1)}, bf16[32,640]{1,0:T(8,128)(2,1)S(1)}, u32[]{:S(2)}, u32[]{:S(2)}) collective-permute-start(bf16[32,640]{1,0:T(8,128)(2,1)S(1)} %get-tuple-element.32), channel_id=1, source_target_pairs={{0,24},{8,0},{16,8},{24,16},{1,25},{9,1},{17,9},{25,17},{2,26},{10... | collective-permute-start | bytes 122888 | tf_op jit(solution)/shard_map/ppermute | solution.py:23
  35.4 5.6 %collective-permute-start.5 = (bf16[32,640]{1,0:T(8,128)(2,1)S(1)}, bf16[32,640]{1,0:T(8,128)(2,1)S(1)}, u32[]{:S(2)}, u32[]{:S(2)}) collective-permute-start(bf16[32,640]{1,0:T(8,128)(2,1)S(1)} %get-tuple-element.33), channel_id=1, source_target_pairs={{0,16},{8,24},{16,0},{24,8},{1,17},{9,25},{17,1},{25,9},{2,18},{10... | collective-permute-start | bytes 122888 | tf_op jit(solution)/shard_map/ppermute | solution.py:23
  35.4 5.7 %collective-permute-start.6 = (bf16[32,640]{1,0:T(8,128)(2,1)S(1)}, bf16[32,640]{1,0:T(8,128)(2,1)S(1)}, u32[]{:S(2)}, u32[]{:S(2)}) collective-permute-start(bf16[32,640]{1,0:T(8,128)(2,1)S(1)} %get-tuple-element.34), channel_id=1, source_target_pairs={{0,8},{8,16},{16,24},{24,0},{1,9},{9,17},{17,25},{25,1},{2,10},{10... | collective-permute-start | bytes 122888 | tf_op jit(solution)/shard_map/ppermute | solution.py:23
  41.0 18.2 %copy-start = (bf16[2048,256]{1,0:T(8,128)(2,1)S(1)}, bf16[2048,256]{1,0:T(8,128)(2,1)}, u32[]{:S(2)}) copy-start(bf16[2048,256]{1,0:T(8,128)(2,1)} %gate_refs_0_.1) | copy-start | bytes 3145732
  41.0 18.3 %copy-start.1 = (bf16[2048,256]{1,0:T(8,128)(2,1)S(1)}, bf16[2048,256]{1,0:T(8,128)(2,1)}, u32[]{:S(2)}) copy-start(bf16[2048,256]{1,0:T(8,128)(2,1)} %up_refs_0_.1) | copy-start | bytes 3145732
  45.8 5.6 %collective-permute-start.7 = (bf16[32,2048]{1,0:T(8,128)(2,1)S(1)}, bf16[32,2048]{1,0:T(8,128)(2,1)S(1)}, u32[]{:S(2)}, u32[]{:S(2)}) collective-permute-start(bf16[32,2048]{1,0:T(8,128)(2,1)S(1)} %get-tuple-element.40.mix_refs_0_), channel_id=1, source_target_pairs={{0,1},{1,2},{2,3},{3,0},{4,5},{5,6},{6,7},{7,4},{8,9},{9,10},{10,1... | collective-permute-start | bytes 393224 | tf_op jit(solution)/shard_map/ppermute | solution.py:23
  47.4 6.6 %collective-permute-start.8 = (bf16[32,2048]{1,0:T(8,128)(2,1)S(1)}, bf16[32,2048]{1,0:T(8,128)(2,1)S(1)}, u32[]{:S(2)}, u32[]{:S(2)}) collective-permute-start(bf16[32,2048]{1,0:T(8,128)(2,1)S(1)} %get-tuple-element.40.mix_refs_0_), channel_id=1, source_target_pairs={{0,2},{1,3},{2,0},{3,1},{4,6},{5,7},{6,4},{7,5},{8,10},{9,11},{10,... | collective-permute-start | bytes 393224 | tf_op jit(solution)/shard_map/ppermute | solution.py:23
  48.4 6.4 %collective-permute-start.9 = (bf16[32,2048]{1,0:T(8,128)(2,1)S(1)}, bf16[32,2048]{1,0:T(8,128)(2,1)S(1)}, u32[]{:S(2)}, u32[]{:S(2)}) collective-permute-start(bf16[32,2048]{1,0:T(8,128)(2,1)S(1)} %get-tuple-element.40.mix_refs_0_), channel_id=1, source_target_pairs={{0,3},{1,0},{2,1},{3,2},{4,7},{5,4},{6,5},{7,6},{8,11},{9,8},{10,9... | collective-permute-start | bytes 393224 | tf_op jit(solution)/shard_map/ppermute | solution.py:23
  55.9 12.4 %all-to-all-start.1 = ((bf16[8,16,512]{2,1,0:T(8,128)(2,1)}), bf16[8,16,512]{2,1,0:T(8,128)(2,1)S(1)}, u32[]{:S(2)}, u32[]{:S(2)}) async-start(bf16[8,16,512]{2,1,0:T(8,128)(2,1)} %bitcast.8), calls=%async_computation.1 | async-start | bytes 262144 | tf_op jit(solution)/shard_map/all_to_all | solution.py:27
  59.2 16.2 %collective-permute-start.10 = (bf16[2048,256]{1,0:T(8,128)(2,1)S(1)}, bf16[2048,256]{1,0:T(8,128)(2,1)}, u32[]{:S(2)}, u32[]{:S(2)}) collective-permute-start(bf16[2048,256]{1,0:T(8,128)(2,1)S(1)} %copy-done), channel_id=1, source_target_pairs={{0,4},{4,0},{1,5},{5,1},{2,6},{6,2},{3,7},{7,3},{8,12},{12,8},{9,1... | collective-permute-start | bytes 3145736 | tf_op jit(solution)/shard_map/ppermute | solution.py:23
  59.4 16.1 %collective-permute-start.11 = (bf16[2048,256]{1,0:T(8,128)(2,1)S(1)}, bf16[2048,256]{1,0:T(8,128)(2,1)}, u32[]{:S(2)}, u32[]{:S(2)}) collective-permute-start(bf16[2048,256]{1,0:T(8,128)(2,1)S(1)} %copy-done.1), channel_id=1, source_target_pairs={{0,4},{4,0},{1,5},{5,1},{2,6},{6,2},{3,7},{7,3},{8,12},{12,8},{9,1... | collective-permute-start | bytes 3145736 | tf_op jit(solution)/shard_map/ppermute | solution.py:23
  59.8 15.6 %collective-permute-start.12 = (bf16[256,2048]{1,0:T(8,128)(2,1)}, bf16[256,2048]{1,0:T(8,128)(2,1)}, u32[]{:S(2)}, u32[]{:S(2)}) collective-permute-start(bf16[256,2048]{1,0:T(8,128)(2,1)} %down_refs_0_.1), channel_id=1, source_target_pairs={{0,4},{4,0},{1,5},{5,1},{2,6},{6,2},{3,7},{7,3},{8,12},{12,8},{9,1... | collective-permute-start | bytes 3145736 | tf_op jit(solution)/shard_map/ppermute | solution.py:23
  69.3 18.3 %all-to-all-start.2 = ((bf16[16,64,512]{2,1,0:T(8,128)(2,1)}), bf16[16,64,512]{2,1,0:T(8,128)(2,1)S(1)}, u32[]{:S(2)}, u32[]{:S(2)}) async-start(bf16[16,64,512]{2,1,0:T(8,128)(2,1)} %bitcast.21), calls=%async_computation.2 | async-start | bytes 2097152 | tf_op jit(solution)/shard_map/all_to_all | solution.py:27
